TPU v7x, 256 devices: a whole 4x4x8 slice. The times are simulated.
256 devices in a mesh: sp: 64 (over z, x, core), tp: 4 (over y).
Axes of the slice: x: 4, y: 4, z: 8, core: 2. Of those that a mesh axis runs over, the one named last changes fastest.
Arguments:
- cotangent: bfloat16 [16384, 2048], P('sp'), may hold values from -16 to 16
- route_ids: int32 [16384, 2], P('sp'), may hold values from 0 to 63, all different within a row; in each aligned block of 256 rows (0 to 255, 256 to 511, ...) at most 16 rows name the same one
- route_weights: float32 [16384, 2], P('sp'), may hold values from 0.2 to 1
- expert_inputs: bfloat16 [64, 1024, 2048], P('sp'), may hold values from -6 to 6
- gate_weight: bfloat16 [64, 2048, 1024], P('sp', None, 'tp'), may hold values from -0.125 to 0.125
- up_weight: bfloat16 [64, 2048, 1024], P('sp', None, 'tp'), may hold values from -0.125 to 0.125
- down_weight: bfloat16 [64, 1024, 2048], P('sp', 'tp'), may hold values from -0.1875 to 0.1875
- out_weight: bfloat16 [2048, 512], P(None, 'tp'), may hold values from -0.25 to 0.25
- gate_in: bfloat16 [16384, 512], P('sp', 'tp'), may hold values from -6 to 6
- conv_sum: bfloat16 [16384, 512], P('sp', 'tp'), may hold values from -6 to 6
- conv_c: bfloat16 [16384, 512], P('sp', 'tp'), may hold values from -6 to 6
- conv_v: bfloat16 [16384, 512], P('sp', 'tp'), may hold values from -6 to 6
- conv_taps: float32 [3, 512], P(None, 'tp'), may hold values from -3 to 3
Outputs:
- grad_input: bfloat16 [16384, 2048], P('sp', 'tp')
- grad_gate: bfloat16 [64, 2048, 1024], P('sp', None, 'tp')
- grad_up: bfloat16 [64, 2048, 1024], P('sp', None, 'tp')
- grad_down: bfloat16 [64, 1024, 2048], P('sp', 'tp')
- grad_out_weight: float32 [2048, 512], P('sp', 'tp')
- grad_gate_in: bfloat16 [16384, 512], P('sp', 'tp')
- grad_conv_c: bfloat16 [16384, 512], P('sp', 'tp')
- grad_conv_v: bfloat16 [16384, 512], P('sp', 'tp')
Inputs may be any that keep to these rules, and one draw needn't show every extreme that they name: `route_ids`: the 2 experts of a token differ. Among the 256 tokens of one index of sp no expert is named more than 16 times, and in every draw some expert is named exactly 16 times by the tokens of some index of sp.
All inputs are finite; a program needn't handle non-finite values.
Results may differ from a plain program's by a relative error of at most 0.012.
Values may be sent and summed in bfloat16 or wider, within the bound.
A program may use at most 128 MiB of HBM per device.

v0:
```python
import jax
import jax.numpy as jnp
from jax import lax
from jax.sharding import PartitionSpec as P

TOP = 2


def split_up(value, dim, peers):
    before, after = (value.shape[:dim], value.shape[dim + 1 :])
    return jnp.moveaxis(value.reshape(*before, peers, -1, *after), dim, 0)


def sum_at_owner(value, axis, dim):
    peers = lax.axis_size(axis)
    pieces = lax.all_to_all(split_up(value, dim, peers), axis, 0, 0, tiled=True)
    return jnp.sum(pieces.astype(jnp.float32), axis=0)


def copy_for_each(value, axis):
    copies = jnp.broadcast_to(value, (lax.axis_size(axis), *value.shape))
    return lax.all_to_all(copies, axis, split_axis=0, concat_axis=0, tiled=True)


def joined_along(pieces, dim):
    shape = list(pieces.shape[1:])
    shape[dim] *= pieces.shape[0]
    return jnp.moveaxis(pieces, 0, dim).reshape(shape)


def collect(value, axis, dim):
    pieces = copy_for_each(value, axis)
    return joined_along(pieces, dim)


def summed_on_arrival(value, axis, dim):
    pieces = split_up(value, dim, lax.axis_size(axis))
    arrived = lax.all_to_all(pieces, axis, split_axis=0, concat_axis=0, tiled=True)
    return arrived.sum(axis=0)


def shifted(block, axis, distance):
    devices = range(lax.axis_size(axis))
    route = [(i - distance, i) for i in devices if i - distance in devices]
    return lax.ppermute(block, axis, route)


def body(
    cotangent,
    route_ids,
    route_weights,
    expert_inputs,
    gate_weight,
    up_weight,
    down_weight,
    out_weight,
    gate_in,
    conv_sum,
    conv_c,
    conv_v,
    conv_taps,
):
    groups = lax.axis_size("sp")
    local_experts = gate_weight.shape[0]
    experts = local_experts * groups
    capacity = expert_inputs.shape[1] // groups
    tok_rows = cotangent.shape[0]
    model_width = cotangent.shape[1]
    targets = route_ids.reshape(-1)
    onehot = (targets[:, None] == jnp.arange(experts, dtype=jnp.int32)[None, :]).astype(jnp.int32)
    before = jnp.cumsum(onehot, axis=0) - onehot
    slot_index = targets * capacity + jnp.sum(before * onehot, axis=1)
    paired = jnp.repeat(cotangent, TOP, axis=0)
    weighted = (route_weights.reshape(-1)[:, None] * paired.astype(jnp.float32)).astype(
        jnp.bfloat16
    )
    owner_row = (
        jnp.full((experts * capacity,), -1, jnp.int32)
        .at[slot_index]
        .set(jnp.arange(targets.shape[0], dtype=jnp.int32))
    )
    outgoing = jnp.where(
        (owner_row >= 0)[:, None],
        jnp.take(weighted, jnp.maximum(owner_row, 0), axis=0),
        jnp.zeros((), jnp.bfloat16),
    )
    outgoing = outgoing.reshape(groups, local_experts * capacity, model_width)
    arrived = lax.all_to_all(outgoing, "sp", split_axis=0, concat_axis=0, tiled=True)
    routed = (
        arrived.reshape(groups, local_experts, capacity, model_width)
        .transpose(1, 0, 2, 3)
        .reshape(local_experts, groups * capacity, model_width)
    )
    pre_gate = jnp.einsum(
        "erd,edf->erf", expert_inputs, gate_weight, preferred_element_type=jnp.float32
    )
    pre_up = jnp.einsum(
        "erd,edf->erf", expert_inputs, up_weight, preferred_element_type=jnp.float32
    )
    gate_sig = jax.nn.sigmoid(pre_gate)
    swish_gate = pre_gate * gate_sig
    hidden = (swish_gate * pre_up).astype(jnp.bfloat16)
    grad_hidden = jnp.einsum(
        "erd,efd->erf", routed, down_weight, preferred_element_type=jnp.float32
    )
    grad_pregate = (grad_hidden * pre_up * gate_sig * (1.0 + pre_gate * (1.0 - gate_sig))).astype(
        jnp.bfloat16
    )
    grad_preup = (grad_hidden * swish_gate).astype(jnp.bfloat16)
    grad_down = jnp.einsum(
        "erf,erd->efd", hidden, routed, preferred_element_type=jnp.float32
    ).astype(jnp.bfloat16)
    grad_gate = jnp.einsum(
        "erd,erf->edf", expert_inputs, grad_pregate, preferred_element_type=jnp.float32
    ).astype(jnp.bfloat16)
    grad_up = jnp.einsum(
        "erd,erf->edf", expert_inputs, grad_preup, preferred_element_type=jnp.float32
    ).astype(jnp.bfloat16)
    partial_in = jnp.einsum(
        "erf,edf->erd", grad_pregate, gate_weight, preferred_element_type=jnp.float32
    )
    partial_in = partial_in + jnp.einsum(
        "erf,edf->erd", grad_preup, up_weight, preferred_element_type=jnp.float32
    )
    rounded = lax.optimization_barrier(partial_in.astype(jnp.bfloat16)).astype(jnp.float32)
    lanes = lax.axis_size("tp")
    lane_cols = model_width // lanes
    summed = sum_at_owner(rounded.astype(jnp.bfloat16), "tp", 2).astype(jnp.bfloat16)
    leaving = (
        summed.reshape(local_experts, groups, capacity, lane_cols)
        .transpose(1, 0, 2, 3)
        .reshape(groups, local_experts * capacity, lane_cols)
    )
    returned = lax.all_to_all(leaving, "sp", split_axis=0, concat_axis=0, tiled=True)
    own_rows = lax.dynamic_slice_in_dim(cotangent, lax.axis_index("tp") * lane_cols, lane_cols, 1)
    returned_sum = jnp.take(
        returned.reshape(experts * capacity, lane_cols), slot_index, axis=0
    ).astype(jnp.float32)
    returned_sum = jnp.sum(returned_sum.reshape(tok_rows, TOP, lane_cols), axis=1)
    grad_input = (own_rows.astype(jnp.float32) + returned_sum).astype(jnp.bfloat16)
    full_mid = collect(grad_input, "tp", 1)
    mixed_rows = (gate_in.astype(jnp.float32) * conv_sum.astype(jnp.float32)).astype(jnp.bfloat16)
    grad_mixed = jnp.dot(full_mid, out_weight, preferred_element_type=jnp.float32)
    grad_out_weight = summed_on_arrival(
        lax.dot_general(
            full_mid, mixed_rows, (((0,), (0,)), ((), ())), preferred_element_type=jnp.float32
        ),
        "sp",
        0,
    )
    grad_gate_in = (grad_mixed * conv_sum.astype(jnp.float32)).astype(jnp.bfloat16)
    grad_sum = grad_mixed * gate_in.astype(jnp.float32)
    next_rows = shifted(grad_sum[:2], "sp", -1)
    extended = jnp.concatenate([grad_sum, next_rows], axis=0)
    grad_prod = (
        conv_taps[0] * extended[2:] + conv_taps[1] * extended[1:-1] + conv_taps[2] * extended[:-2]
    )
    grad_conv_c = (grad_prod * conv_v.astype(jnp.float32)).astype(jnp.bfloat16)
    grad_conv_v = (grad_prod * conv_c.astype(jnp.float32)).astype(jnp.bfloat16)
    return (
        grad_input,
        grad_gate,
        grad_up,
        grad_down,
        grad_out_weight,
        grad_gate_in,
        grad_conv_c,
        grad_conv_v,
    )


def solution(mesh):
    placed = (
        P("sp", None),
        P("sp", None),
        P("sp", None),
        P("sp", None, None),
        P("sp", None, "tp"),
        P("sp", None, "tp"),
        P("sp", "tp", None),
        P(None, "tp"),
        P("sp", "tp"),
        P("sp", "tp"),
        P("sp", "tp"),
        P("sp", "tp"),
        P(None, "tp"),
    )
    return jax.shard_map(
        body,
        mesh=mesh,
        in_specs=placed,
        out_specs=(
            P("sp", "tp"),
            P("sp", None, "tp"),
            P("sp", None, "tp"),
            P("sp", "tp", None),
            P("sp", "tp"),
            P("sp", "tp"),
            P("sp", "tp"),
            P("sp", "tp"),
        ),
        check_vma=False,
    )
```

profile of v0, /device:TPU:17, one launch (start us, length us, event | category | flops | bytes accessed | tf_op | source)
XLA Modules:
  0.0 297.3 jit_solution(16947683690868798605)
XLA Ops:
  0.6 0.8 broadcast_multiply_fusion
  1.4 0.8 copy.42
  2.2 0.1 eq.26
  2.4 0.1 reshape.174
  2.7 0.1 mul.112
  2.8 1.2 reduce-window.6
  4.0 0.2 slice_reduce_fusion
  4.5 2.4 scatter_custom_fusion
  7.1 0.8 copy.48
  7.9 0.1 mul.113
  8.1 5.3 %broadcast_in_dim.56 = f32[256,2,2048]{2,1,0:T(2,128)} broadcast(bf16[256,2048]{1,0:T(8,128)(2,1)} %param.13), dimensions={0,2} | broadcast | bytes 5242880 | tf_op jit(solution)/shard_map/broadcast_in_dim | solution.py:73
  13.4 6.1 %convert_element_type.103 = f32[512,2048]{1,0:T(8,128)} reshape(f32[256,2,2048]{2,1,0:T(2,128)} %broadcast_in_dim.56) | data formatting | bytes 8388608 | tf_op jit(solution)/shard_map/convert_element_type | solution.py:74
  19.5 2.5 multiply_convert_fusion
  22.0 6.0 %gather_fusion = bf16[1024,2048]{1,0:T(8,128)(2,1)} fusion(bf16[512,2048]{1,0:T(8,128)(2,1)S(1)} %multiply_convert_fusion, s32[1024]{0:T(1024)S(1)} %maximum_clamp_fusion), kind=kCustom, calls=%fused_computation | custom fusion | bytes 8392704 | tf_op jit(solution)/shard_map/jit(_take)/gather | solution.py:84
  28.0 3.9 %select_select_fusion = bf16[64,16,2048]{2,1,0:T(8,128)(2,1)} fusion(bf16[64,16,2048]{2,1,0:T(8,128)(2,1)} %bitcast.103, pred[64,16]{1,0:T(8,128)(4,1)S(1)} %broadcast_in_dim.54, pred[64,16]{1,0:T(8,128)(4,1)S(1)} %broadcast_in_dim.52), kind=kLoop, calls=%fused_computation.13 | loop fusion | flops 4194304 | bytes 8390656 | tf_op jit(solution)/shard_map/jit(_where)/select_n | solution.py:82
  31.9 12.4 %all-to-all-start = ((bf16[64,16,2048]{2,1,0:T(8,128)(2,1)}), bf16[64,16,2048]{2,1,0:T(8,128)(2,1)}, u32[]{:S(2)}, u32[]{:S(2)}) async-start(bf16[64,16,2048]{2,1,0:T(8,128)(2,1)} %select_select_fusion), calls=%async_computation | async-start | bytes 8388608 | tf_op jit(solution)/shard_map/all_to_all | solution.py:88
  44.3 4.6 %fusion.4 = f32[1024,256]{1,0:T(8,128)} fusion(bf16[1,1024,2048]{2,1,0:T(8,128)(2,1)} %param.16, bf16[1,2048,256]{2,1,0:T(8,128)(2,1)S(1)} %copy-done), kind=kOutput, calls=%fused_computation.9 | convolution fusion | flops 1073741824 | bytes 6291456 | tf_op jit(solution)/shard_map/erd,edf->erf/dot_general | solution.py:94
  48.8 2.2 fusion.6
  51.1 87.9 %all-to-all-done = bf16[64,16,2048]{2,1,0:T(8,128)(2,1)} async-done(((bf16[64,16,2048]{2,1,0:T(8,128)(2,1)}), bf16[64,16,2048]{2,1,0:T(8,128)(2,1)}, u32[]{:S(2)}, u32[]{:S(2)}) %all-to-all-start) | async-done | bytes 4194336 | tf_op jit(solution)/shard_map/all_to_all | solution.py:88
  138.9 4.3 %multiply_convert_fusion.2 = (bf16[1024,256]{1,0:T(8,128)(2,1)S(1)}, bf16[1024,256]{1,0:T(8,128)(2,1)S(1)}) fusion(f32[1024,256]{1,0:T(8,128)} %fusion.4, f32[1024,256]{1,0:T(8,128)} %fusion.6, bf16[1024,2048]{1,0:T(8,128)(2,1)} %bitcast.4, bf16[1,256,2048]{2,1,0:T(8,128)(2,1)S(1)} %copy-done.16), kind=kOutput, calls=%fused_computation.31 | convolution fusion | flops 1077149696 | bytes 8388608 | tf_op jit(solution)/shard_map/erd,efd->erf/dot_general | solution.py:103
  143.3 1.3 fusion.22
  144.6 1.3 fusion.8
  145.9 0.4 copy.57
  146.3 48.0 %all_to_all.25 = bf16[4,1,1024,512]{3,2,1,0:T(8,128)(2,1)} all-to-all(bf16[4,1,1024,512]{3,2,1,0:T(8,128)(2,1)S(1)} %bitcast.105), channel_id=1, replica_groups=mesh['sp'=64,'tp'=4] {'tp'}, dimensions={0} | all-to-all | bytes 8388608 | tf_op jit(solution)/shard_map/all_to_all | solution.py:16
  194.3 4.1 %reduce_sum.46 = bf16[1024,512]{1,0:T(8,128)(2,1)} reduce(bf16[4,1,1024,512]{3,2,1,0:T(8,128)(2,1)} %all_to_all.25, bf16[]{:T(256)} %constant.55.clone.1), dimensions={0,1}, to_apply=%region_4.5 | reduce | flops 1572864 | bytes 5242882 | tf_op jit(solution)/shard_map/reduce_sum | solution.py:17
  198.4 9.7 %all-to-all-start.2 = ((bf16[64,16,512]{2,1,0:T(8,128)(2,1)}), bf16[64,16,512]{2,1,0:T(8,128)(2,1)S(1)}, u32[]{:S(2)}, u32[]{:S(2)}) async-start(bf16[64,16,512]{2,1,0:T(8,128)(2,1)} %bitcast.11), calls=%async_computation.2 | async-start | bytes 2097152 | tf_op jit(solution)/shard_map/all_to_all | solution.py:134
  208.4 0.2 copy.46
  208.6 27.7 %all-to-all-done.2 = bf16[64,16,512]{2,1,0:T(8,128)(2,1)S(1)} async-done(((bf16[64,16,512]{2,1,0:T(8,128)(2,1)}), bf16[64,16,512]{2,1,0:T(8,128)(2,1)S(1)}, u32[]{:S(2)}, u32[]{:S(2)}) %all-to-all-start.2) | async-done | bytes 1048608 | tf_op jit(solution)/shard_map/all_to_all | solution.py:134
  236.3 2.0 gather_fusion.1
  238.3 0.2 gather.15
  238.5 1.7 convert_reduce_fusion
  240.2 1.0 add_convert_fusion.1
  241.4 1.0 broadcast_in_dim.61
  242.4 5.9 %all-to-all-start.3 = ((bf16[4,256,512]{1,2,0:T(8,128)(2,1)}), bf16[4,256,512]{1,2,0:T(8,128)(2,1)S(1)}, u32[]{:S(2)}, u32[]{:S(2)}) async-start(bf16[4,256,512]{1,2,0:T(8,128)(2,1)} %broadcast_in_dim.61), calls=%async_computation.3 | async-start | bytes 2097152 | tf_op jit(solution)/shard_map/all_to_all | solution.py:22
  248.3 11.4 %all-to-all-done.3 = bf16[4,256,512]{1,2,0:T(8,128)(2,1)S(1)} async-done(((bf16[4,256,512]{1,2,0:T(8,128)(2,1)}), bf16[4,256,512]{1,2,0:T(8,128)(2,1)S(1)}, u32[]{:S(2)}, u32[]{:S(2)}) %all-to-all-start.3) | async-done | bytes 1048608 | tf_op jit(solution)/shard_map/all_to_all | solution.py:22
  259.7 1.4 fusion.43
  261.1 7.3 %all-to-all-start.4 = ((f32[64,32,128]{2,1,0:T(8,128)}), f32[64,32,128]{2,1,0:T(8,128)S(1)}, u32[]{:S(2)}, u32[]{:S(2)}) async-start(f32[64,32,128]{2,1,0:T(8,128)} %fusion.43), calls=%async_computation.4 | async-start | bytes 2097152 | tf_op jit(solution)/shard_map/all_to_all | solution.py:38
  268.5 3.8 %fusion.16 = bf16[1,2048,256]{1,2,0:T(8,128)(2,1)S(1)} fusion(bf16[1024,256]{1,0:T(8,128)(2,1)} %copy-done.6, bf16[1,1024,2048]{2,1,0:T(8,128)(2,1)} %param.16), kind=kOutput, calls=%fused_computation.20 | convolution fusion | flops 1074266112 | bytes 5767168 | tf_op jit(solution)/shard_map/erd,erf->edf/dot_general | solution.py:116
  272.3 4.7 %fusion.15 = bf16[1,256,2048]{2,1,0:T(8,128)(2,1)} fusion(bf16[1024,2048]{1,0:T(8,128)(2,1)} %bitcast.4, f32[1024,256]{1,0:T(8,128)S(1)} %copy-done.18, f32[1024,256]{1,0:T(8,128)S(1)} %copy-done.17), kind=kOutput, calls=%fused_computation.19 | convolution fusion | flops 1075838976 | bytes 7340032 | tf_op jit(solution)/shard_map/erf,erd->efd/dot_general | solution.py:110
  277.0 1.1 convert_multiply_fusion.2
  278.1 2.5 collective-permute-start
  280.6 2.2 fusion.19
  282.9 1.3 copy.52
  284.2 2.3 copy.51
  286.5 0.7 multiply_convert_fusion.5
  287.2 0.6 multiply_convert_fusion.6
  287.8 8.8 %all-to-all-done.4 = f32[64,32,128]{2,1,0:T(8,128)S(1)} async-done(((f32[64,32,128]{2,1,0:T(8,128)}), f32[64,32,128]{2,1,0:T(8,128)S(1)}, u32[]{:S(2)}, u32[]{:S(2)}) %all-to-all-start.4) | async-done | bytes 1048608 | tf_op jit(solution)/shard_map/all_to_all | solution.py:38
  296.6 0.7 reduce_sum.48
  (57 shorter events, 1.0 us)
Async XLA Ops:
  0.6 43.6 %copy-start = (bf16[1,2048,256]{2,1,0:T(8,128)(2,1)S(1)}, bf16[1,2048,256]{2,1,0:T(8,128)(2,1)}, u32[]{:S(2)}) copy-start(bf16[1,2048,256]{2,1,0:T(8,128)(2,1)} %param.17) | copy-start | bytes 3145732
  31.9 107.1 %all-to-all-start = ((bf16[64,16,2048]{2,1,0:T(8,128)(2,1)}), bf16[64,16,2048]{2,1,0:T(8,128)(2,1)}, u32[]{:S(2)}, u32[]{:S(2)}) async-start(bf16[64,16,2048]{2,1,0:T(8,128)(2,1)} %select_select_fusion), calls=%async_computation | async-start | bytes 8388608 | tf_op jit(solution)/shard_map/all_to_all | solution.py:88
  44.3 4.6 %copy-start.2 = (bf16[1,2048,256]{2,1,0:T(8,128)(2,1)S(1)}, bf16[1,2048,256]{2,1,0:T(8,128)(2,1)}, u32[]{:S(2)}) copy-start(bf16[1,2048,256]{2,1,0:T(8,128)(2,1)} %param.18) | copy-start | bytes 3145732
  44.3 4.6 %copy-start.14 = (bf16[1,1024,2048]{2,1,0:T(8,128)(2,1)S(1)}, bf16[1,1024,2048]{2,1,0:T(8,128)(2,1)}, u32[]{:S(2)}) copy-start(bf16[1,1024,2048]{2,1,0:T(8,128)(2,1)} %param.16) | copy-start | bytes 12582916
  48.8 90.1 %copy-start.16 = (bf16[1,256,2048]{2,1,0:T(8,128)(2,1)S(1)}, bf16[1,256,2048]{2,1,0:T(8,128)(2,1)}, u32[]{:S(2)}) copy-start(bf16[1,256,2048]{2,1,0:T(8,128)(2,1)} %param.19) | copy-start | bytes 3145732
  143.3 1.3 copy-start.4
  143.3 1.3 copy-start.6
  194.3 14.1 %copy-start.12 = (s32[256,2]{0,1:T(2,128)S(1)}, s32[256,2]{0,1:T(2,128)}, u32[]{:S(2)}) copy-start(s32[256,2]{0,1:T(2,128)} %param.14) | copy-start | bytes 6148
  198.4 37.9 %all-to-all-start.2 = ((bf16[64,16,512]{2,1,0:T(8,128)(2,1)}), bf16[64,16,512]{2,1,0:T(8,128)(2,1)S(1)}, u32[]{:S(2)}, u32[]{:S(2)}) async-start(bf16[64,16,512]{2,1,0:T(8,128)(2,1)} %bitcast.11), calls=%async_computation.2 | async-start | bytes 2097152 | tf_op jit(solution)/shard_map/all_to_all | solution.py:134
  238.2 10.1 %copy-start.13 = (f32[3,128]{1,0:T(4,128)S(1)}, f32[3,128]{1,0:T(4,128)}, u32[]{:S(2)}) copy-start(f32[3,128]{1,0:T(4,128)} %param.25) | copy-start | bytes 4612
  238.3 21.5 %copy-start.8 = (bf16[256,128]{1,0:T(8,128)(2,1)S(1)}, bf16[256,128]{1,0:T(8,128)(2,1)}, u32[]{:S(2)}) copy-start(bf16[256,128]{1,0:T(8,128)(2,1)} %param.22) | copy-start | bytes 196612
  238.3 21.5 %copy-start.9 = (bf16[256,128]{1,0:T(8,128)(2,1)S(1)}, bf16[256,128]{1,0:T(8,128)(2,1)}, u32[]{:S(2)}) copy-start(bf16[256,128]{1,0:T(8,128)(2,1)} %param.21) | copy-start | bytes 196612
  241.2 31.0 %copy-start.3 = (bf16[256,512]{1,0:T(8,128)(2,1)}, bf16[256,512]{1,0:T(8,128)(2,1)S(1)}, u32[]{:S(2)}) copy-start(bf16[256,512]{1,0:T(8,128)(2,1)S(1)} %add_convert_fusion.1) | copy-start | bytes 786436
  242.4 17.3 %all-to-all-start.3 = ((bf16[4,256,512]{1,2,0:T(8,128)(2,1)}), bf16[4,256,512]{1,2,0:T(8,128)(2,1)S(1)}, u32[]{:S(2)}, u32[]{:S(2)}) async-start(bf16[4,256,512]{1,2,0:T(8,128)(2,1)} %broadcast_in_dim.61), calls=%async_computation.3 | async-start | bytes 2097152 | tf_op jit(solution)/shard_map/all_to_all | solution.py:22
  261.1 35.5 %all-to-all-start.4 = ((f32[64,32,128]{2,1,0:T(8,128)}), f32[64,32,128]{2,1,0:T(8,128)S(1)}, u32[]{:S(2)}, u32[]{:S(2)}) async-start(f32[64,32,128]{2,1,0:T(8,128)} %fusion.43), calls=%async_computation.4 | async-start | bytes 2097152 | tf_op jit(solution)/shard_map/all_to_all | solution.py:38
  268.5 3.8 %copy-start.17 = (f32[1024,256]{1,0:T(8,128)S(1)}, f32[1024,256]{1,0:T(8,128)}, u32[]{:S(2)}) copy-start(f32[1024,256]{1,0:T(8,128)} %fusion.4) | copy-start | bytes 3145732
  268.5 3.8 %copy-start.18 = (f32[1024,256]{1,0:T(8,128)S(1)}, f32[1024,256]{1,0:T(8,128)}, u32[]{:S(2)}) copy-start(f32[1024,256]{1,0:T(8,128)} %fusion.6) | copy-start | bytes 3145732
  272.3 4.7 %copy-start.7 = (bf16[2048,128]{1,0:T(8,128)(2,1)S(1)}, bf16[2048,128]{1,0:T(8,128)(2,1)}, u32[]{:S(2)}) copy-start(bf16[2048,128]{1,0:T(8,128)(2,1)} %param.20) | copy-start | bytes 1572868
  272.3 8.3 %copy-start.5 = (bf16[1024,256]{1,0:T(8,128)(2,1)S(1)}, bf16[1024,256]{1,0:T(8,128)(2,1)}, u32[]{:S(2)}) copy-start(bf16[1024,256]{1,0:T(8,128)(2,1)} %copy-done.4) | copy-start | bytes 1572868
  272.3 8.3 %copy-start.15 = (bf16[1,1024,2048]{2,1,0:T(8,128)(2,1)S(1)}, bf16[1,1024,2048]{2,1,0:T(8,128)(2,1)}, u32[]{:S(2)}) copy-start(bf16[1,1024,2048]{2,1,0:T(8,128)(2,1)} %param.16) | copy-start | bytes 12582916
  278.1 8.3 %copy-start.10 = (bf16[256,128]{1,0:T(8,128)(2,1)S(1)}, bf16[256,128]{1,0:T(8,128)(2,1)}, u32[]{:S(2)}) copy-start(bf16[256,128]{1,0:T(8,128)(2,1)} %param.23) | copy-start | bytes 196612
  278.1 9.0 %copy-start.11 = (bf16[256,128]{1,0:T(8,128)(2,1)S(1)}, bf16[256,128]{1,0:T(8,128)(2,1)}, u32[]{:S(2)}) copy-start(bf16[256,128]{1,0:T(8,128)(2,1)} %param.24) | copy-start | bytes 196612
  278.1 8.3 %collective-permute-start = (f32[2,128]{1,0:T(2,128)S(1)}, f32[2,128]{1,0:T(2,128)S(1)}, u32[]{:S(2)}, u32[]{:S(2)}) collective-permute-start(f32[2,128]{1,0:T(2,128)S(1)} %slice.37), channel_id=1, source_target_pairs={{4,0},{8,4},{12,8},{16,12},{20,16},{24,20},{28,24},{32,28},{36,32}... | collective-permute-start | bytes 3080 | tf_op jit(solution)/shard_map/ppermute | solution.py:45
  280.6 16.7 %copy-start.1 = (bf16[1,2048,256]{2,1,0:T(8,128)(2,1)S(1)}, bf16[1,2048,256]{2,1,0:T(8,128)(2,1)}, u32[]{:S(2)}) copy-start(bf16[1,2048,256]{2,1,0:T(8,128)(2,1)} %param.17) | copy-start | bytes 3145732
where the time goes:
time: 302 us; the launch traced here: 297 us
  waiting for transfers between devices  136 us (45%)
  blocking collectives  48 us (16%)
  starting transfers between devices  37.8 us (13%)
  local copies, waits for them, and re-layouts  30.4 us (10%)
  matrix products  26.9 us (9%)
  other arithmetic  17.4 us (6%)
    all_to_all x1, waiting for transfers between devices, body(): lax.all_to_all(outgoing, 'sp', split_axis=0, concat_axis=0, tiled=True)  87.9 us
    all_to_all x1, blocking collectives, sum_at_owner(): pieces = lax.all_to_all(split_up(value, dim, peers), axis, 0, 0, tiled=True)  48 us
    all_to_all x1, waiting for transfers between devices, body(): lax.all_to_all(leaving, 'sp', split_axis=0, concat_axis=0, tiled=True)  27.7 us
    all_to_all x1, starting transfers between devices, body(): lax.all_to_all(outgoing, 'sp', split_axis=0, concat_axis=0, tiled=True)  12.4 us
    all_to_all x1, waiting for transfers between devices, copy_for_each(): return lax.all_to_all(copies, axis, split_axis=0, concat_axis=0, tiled=True)  11.4 us
    all_to_all x1, starting transfers between devices, body(): lax.all_to_all(leaving, 'sp', split_axis=0, concat_axis=0, tiled=True)  9.73 us
    all_to_all x1, waiting for transfers between devices, summed_on_arrival(): lax.all_to_all(pieces, axis, split_axis=0, concat_axis=0, tiled=True)  8.83 us
    all_to_all x1, starting transfers between devices, summed_on_arrival(): lax.all_to_all(pieces, axis, split_axis=0, concat_axis=0, tiled=True)  7.33 us
  transfers between devices with their start and end apart: 5, of which 4 were waited for; matrix products, arithmetic and copies ran while one was open for 8% of the time, Pallas kernels for 0%

commit v1 on v0

v1 whole, which is shorter than its diff:
```python
import functools

import jax
import jax.numpy as jnp
from jax import lax
from jax.experimental import pallas as pl
from jax.experimental.pallas import tpu as pltpu
from jax.sharding import PartitionSpec as P

TOP = 2
MESH = pl.DeviceIdType.MESH
F32 = jnp.float32
BF16 = jnp.bfloat16


def expert_kernel(
    dims,
    out_ref,
    x_hbm,
    gate_hbm,
    up_hbm,
    down_hbm,
    returned,
    g_gate,
    g_up,
    g_down,
    x_v,
    gate_v,
    up_v,
    down_v,
    routed,
    part,
    rs1a,
    rs1b,
    rs2a,
    rs2b,
    ret_src,
    swish_s,
    slope_s,
    hidden_s,
    gpg_s,
    gpu_s,
    load_sem,
    send_z,
    recv_z,
    send_y,
    recv_y,
    send_r,
    recv_r,
):
    sps, tps, chunks, cap = dims
    group = sps // chunks
    rows_c = group * cap
    half = rows_c // 2
    cols = out_ref.shape[1]
    me = lax.axis_index("sp")
    q = lax.axis_index("tp")
    z = me // group
    g = me % group
    up_q = (q + 1) % tps
    dn_q = (q + tps - 1) % tps
    far_q = (q + 2) % tps

    loads = [
        pltpu.make_async_copy(src, dst, load_sem.at[n])
        for n, (src, dst) in enumerate(
            ((x_hbm, x_v), (gate_hbm, gate_v), (up_hbm, up_v), (down_hbm, down_v))
        )
    ]
    for load in loads:
        load.start()

    barrier = pltpu.get_barrier_semaphore()

    def greet(k, carry):
        pl.semaphore_signal(
            barrier, inc=1, device_id=((me + k) % sps, q), device_id_type=MESH
        )
        return carry

    lax.fori_loop(1, sps, greet, 0)
    for peer in (up_q, dn_q):
        pl.semaphore_signal(barrier, inc=1, device_id=(me, peer), device_id_type=MESH)
    pl.semaphore_wait(barrier, sps - 1 + 2)

    def offset(i):
        return ((i + 1) // 2) * (2 * (i % 2) - 1)

    def chunk_start(i):
        return ((z - offset(i) + chunks) % chunks) * rows_c

    def block_copy(i, k):
        peer = ((z + offset(i) + chunks) % chunks) * group + (g + k) % group
        return pltpu.make_async_remote_copy(
            src_ref=out_ref.at[pl.ds(pl.multiple_of(peer * cap, cap), cap), :],
            dst_ref=routed.at[q, pl.ds(pl.multiple_of(me * cap, cap), cap), :],
            send_sem=send_z.at[i],
            recv_sem=recv_z.at[i],
            device_id=(peer, q),
            device_id_type=MESH,
        )

    def send_first(k, carry):
        block_copy(0, k).start()
        return carry

    lax.fori_loop(1, group, send_first, 0)

    def send_chunk(i, carry):
        def send_one(k, inner):
            block_copy(i, k).start()
            return inner

        return lax.fori_loop(0, group, send_one, carry)

    lax.fori_loop(1, chunks, send_chunk, 0)
    own = pl.ds(pl.multiple_of(me * cap, cap), cap)
    routed[q, own, :] = out_ref[own, :]

    for load in loads:
        load.wait()
    pre_rows = 2 * rows_c

    def forward(b, carry):
        rows = pl.ds(pl.multiple_of(b * pre_rows, pre_rows), pre_rows)
        pre_gate = jnp.dot(x_v[rows, :], gate_v[...], preferred_element_type=F32)
        pre_up = jnp.dot(x_v[rows, :], up_v[...], preferred_element_type=F32)
        sig = jax.nn.sigmoid(pre_gate)
        swish = pre_gate * sig
        swish_s[rows, :] = swish
        slope_s[rows, :] = pre_up * sig * (1.0 + pre_gate * (1.0 - sig))
        hidden_s[rows, :] = (swish * pre_up).astype(BF16)
        return carry

    lax.fori_loop(0, sps * cap // pre_rows, forward, 0)

    def at(i, first=0, size=None):
        return pl.ds(pl.multiple_of(chunk_start(i) + first, half), size or rows_c)

    def y_copy(src, dst, kind, i, peer):
        return pltpu.make_async_remote_copy(
            src_ref=src,
            dst_ref=dst,
            send_sem=send_y.at[kind, i],
            recv_sem=recv_y.at[kind, i],
            device_id=(me, peer),
            device_id_type=MESH,
        )

    def gather_up(i):
        ref = routed.at[q, at(i), :]
        return y_copy(ref, ref, 0, i, up_q)

    def gather_dn(i):
        ref = routed.at[q, at(i), :]
        return y_copy(ref, ref, 1, i, dn_q)

    def pass_up(i):
        ref = routed.at[dn_q, at(i, 0, half), :]
        return y_copy(ref, ref, 2, i, up_q)

    def pass_dn(i):
        ref = routed.at[up_q, at(i, half, half), :]
        return y_copy(ref, ref, 3, i, dn_q)

    def first_up(i):
        return y_copy(part.at[far_q, at(i, 0, half), :], rs1a.at[i], 4, i, up_q)

    def first_dn(i):
        return y_copy(part.at[far_q, at(i, half, half), :], rs1b.at[i], 5, i, dn_q)

    def last_up(i):
        return y_copy(part.at[up_q, at(i), :], rs2a.at[i], 6, i, up_q)

    def last_dn(i):
        return y_copy(part.at[dn_q, at(i), :], rs2b.at[i], 7, i, dn_q)

    every = (gather_up, gather_dn, pass_up, pass_dn, first_up, first_dn, last_up, last_dn)

    def wait_z(i, count):
        rows = pl.ds(0, count * cap)
        pltpu.make_async_remote_copy(
            src_ref=out_ref.at[rows, :],
            dst_ref=routed.at[q, rows, :],
            send_sem=send_z.at[i],
            recv_sem=recv_z.at[i],
            device_id=(me, up_q),
            device_id_type=MESH,
        ).wait_recv()

    def stage_gather(i):
        @pl.when(i == 0)
        def _():
            wait_z(i, group - 1)

        @pl.when(i > 0)
        def _():
            wait_z(i, group)

        gather_up(i).start()
        gather_dn(i).start()

    def stage_pass(i):
        gather_up(i).wait_recv()
        pass_up(i).start()
        gather_dn(i).wait_recv()
        pass_dn(i).start()

    def stage_compute(i):
        pass_up(i).wait_recv()
        pass_dn(i).wait_recv()
        rows = at(i)
        grad_hidden = jnp.zeros((rows_c, down_v.shape[0]), F32)
        for lane in range(tps):
            grad_hidden += lax.dot_general(
                routed[lane, rows, :],
                down_v[:, lane * cols : (lane + 1) * cols],
                (((1,), (1,)), ((), ())),
                preferred_element_type=F32,
            )
        gpg = (grad_hidden * slope_s[rows, :]).astype(BF16)
        gpu = (grad_hidden * swish_s[rows, :]).astype(BF16)
        gpg_s[rows, :] = gpg
        gpu_s[rows, :] = gpu
        for lane in range(tps):
            span = slice(lane * cols, (lane + 1) * cols)
            piece = lax.dot_general(
                gpg, gate_v[span, :], (((1,), (1,)), ((), ())), preferred_element_type=F32
            )
            piece += lax.dot_general(
                gpu, up_v[span, :], (((1,), (1,)), ((), ())), preferred_element_type=F32
            )
            part[lane, rows, :] = piece.astype(BF16)
        first_up(i).start()
        first_dn(i).start()

    def stage_first(i):
        lower, upper = at(i, 0, half), at(i, half, half)
        first_up(i).wait_recv()
        part[up_q, lower, :] = (
            part[up_q, lower, :].astype(F32) + rs1a[i].astype(F32)
        ).astype(BF16)
        last_up(i).start()
        first_dn(i).wait_recv()
        part[dn_q, upper, :] = (
            part[dn_q, upper, :].astype(F32) + rs1b[i].astype(F32)
        ).astype(BF16)
        last_dn(i).start()

    def return_copy(i, k):
        source = ((z - offset(i) + chunks) % chunks) * group + (g + k) % group
        return pltpu.make_async_remote_copy(
            src_ref=ret_src.at[pl.ds(pl.multiple_of(source * cap, cap), cap), :],
            dst_ref=returned.at[own, :],
            send_sem=send_r,
            recv_sem=recv_r,
            device_id=(source, q),
            device_id_type=MESH,
        )

    def stage_return(i):
        rows = at(i)
        last_up(i).wait_recv()
        last_dn(i).wait_recv()
        total = part[q, rows, :].astype(F32) + rs2a[i].astype(F32) + rs2b[i].astype(F32)
        ret_src[rows, :] = total.astype(BF16)

        @pl.when(i > 0)
        def _():
            return_copy(i, 0).start()

        def send_one(k, carry):
            return_copy(i, k).start()
            return carry

        lax.fori_loop(1, group, send_one, 0)

    stages = (stage_gather, stage_pass, stage_compute, stage_first, stage_return)

    def step(t, carry):
        for depth, stage in reversed(tuple(enumerate(stages))):
            i = t - depth

            @pl.when((i >= 0) & (i < chunks))
            def _():
                stage(i)

        return carry

    lax.fori_loop(0, chunks + len(stages) - 1, step, 0)
    returned[own, :] = ret_src[own, :]

    contract0 = (((0,), (0,)), ((), ()))
    for lane in range(tps):
        span = slice(lane * cols, (lane + 1) * cols)
        g_down[:, span] = lax.dot_general(
            hidden_s[...], routed[lane], contract0, preferred_element_type=F32
        ).astype(BF16)
        g_gate[span, :] = lax.dot_general(
            x_v[:, span], gpg_s[...], contract0, preferred_element_type=F32
        ).astype(BF16)
        g_up[span, :] = lax.dot_general(
            x_v[:, span], gpu_s[...], contract0, preferred_element_type=F32
        ).astype(BF16)

    def drain(i, carry):
        for copy in every:
            copy(i).wait_send()
        return carry

    lax.fori_loop(0, chunks, drain, 0)

    def drain_z(i, count):
        rows = pl.ds(0, count * cap)
        pltpu.make_async_remote_copy(
            src_ref=out_ref.at[rows, :],
            dst_ref=routed.at[q, rows, :],
            send_sem=send_z.at[i],
            recv_sem=recv_z.at[i],
            device_id=(me, up_q),
            device_id_type=MESH,
        ).wait_send()

    drain_z(0, group - 1)

    def drain_rest(i, carry):
        drain_z(i, group)
        return carry

    lax.fori_loop(1, chunks, drain_rest, 0)
    rest = pl.ds(0, (sps - 1) * cap)
    final = pltpu.make_async_remote_copy(
        src_ref=ret_src.at[rest, :],
        dst_ref=returned.at[rest, :],
        send_sem=send_r,
        recv_sem=recv_r,
        device_id=(me, up_q),
        device_id_type=MESH,
    )
    final.wait_send()
    final.wait_recv()


def run_experts(dims, outgoing, x, gate, up, down):
    sps, tps, chunks, cap = dims
    rows, cols = outgoing.shape
    width, units = gate.shape
    rows_c = rows // chunks
    vmem = pl.BlockSpec(memory_space=pltpu.VMEM)
    hbm = pl.BlockSpec(memory_space=pltpu.HBM)
    scratch = [
        pltpu.VMEM((rows, width), BF16),
        pltpu.VMEM((width, units), BF16),
        pltpu.VMEM((width, units), BF16),
        pltpu.VMEM((units, width), BF16),
        pltpu.VMEM((tps, rows, cols), BF16),
        pltpu.VMEM((tps, rows, cols), BF16),
        pltpu.VMEM((chunks, rows_c // 2, cols), BF16),
        pltpu.VMEM((chunks, rows_c // 2, cols), BF16),
        pltpu.VMEM((chunks, rows_c, cols), BF16),
        pltpu.VMEM((chunks, rows_c, cols), BF16),
        pltpu.VMEM((rows, cols), BF16),
        pltpu.VMEM((rows, units), F32),
        pltpu.VMEM((rows, units), F32),
        pltpu.VMEM((rows, units), BF16),
        pltpu.VMEM((rows, units), BF16),
        pltpu.VMEM((rows, units), BF16),
        pltpu.SemaphoreType.DMA((4,)),
        pltpu.SemaphoreType.DMA((chunks,)),
        pltpu.SemaphoreType.DMA((chunks,)),
        pltpu.SemaphoreType.DMA((8, chunks)),
        pltpu.SemaphoreType.DMA((8, chunks)),
        pltpu.SemaphoreType.DMA,
        pltpu.SemaphoreType.DMA,
    ]
    return pl.pallas_call(
        functools.partial(expert_kernel, dims),
        out_shape=(
            jax.ShapeDtypeStruct((rows, cols), BF16),
            jax.ShapeDtypeStruct((width, units), BF16),
            jax.ShapeDtypeStruct((width, units), BF16),
            jax.ShapeDtypeStruct((units, width), BF16),
        ),
        in_specs=[vmem, hbm, hbm, hbm, hbm],
        out_specs=(vmem, vmem, vmem, vmem),
        scratch_shapes=scratch,
        compiler_params=pltpu.CompilerParams(
            collective_id=0, has_side_effects=True, vmem_limit_bytes=60 * 1024 * 1024
        ),
        name="experts",
    )(outgoing, x, gate, up, down)


def split_up(value, dim, peers):
    before, after = (value.shape[:dim], value.shape[dim + 1 :])
    return jnp.moveaxis(value.reshape(*before, peers, -1, *after), dim, 0)


def collect(value, axis, dim):
    copies = jnp.broadcast_to(value, (lax.axis_size(axis), *value.shape))
    pieces = lax.all_to_all(copies, axis, split_axis=0, concat_axis=0, tiled=True)
    shape = list(value.shape)
    shape[dim] *= pieces.shape[0]
    return jnp.moveaxis(pieces, 0, dim).reshape(shape)


def summed_on_arrival(value, axis, dim):
    pieces = split_up(value, dim, lax.axis_size(axis))
    arrived = lax.all_to_all(pieces, axis, split_axis=0, concat_axis=0, tiled=True)
    return arrived.astype(F32).sum(axis=0)


def shifted(block, axis, distance):
    devices = range(lax.axis_size(axis))
    route = [(i - distance, i) for i in devices if i - distance in devices]
    return lax.ppermute(block, axis, route)


def routing(route_ids, route_weights, experts, capacity):
    tokens = route_ids.shape[0]
    ids = route_ids.T
    weights = route_weights.T
    names = lax.broadcasted_iota(jnp.int32, (experts, tokens), 0)
    first, second = names == ids[0][None, :], names == ids[1][None, :]
    weight = jnp.where(first, weights[0][None, :], 0.0) + jnp.where(
        second, weights[1][None, :], 0.0
    )
    named = first | second
    earlier = lax.broadcasted_iota(jnp.int32, (tokens, tokens), 0) < lax.broadcasted_iota(
        jnp.int32, (tokens, tokens), 1
    )
    rank = jnp.dot(named.astype(BF16), earlier.astype(BF16), preferred_element_type=F32)
    rank = jnp.where(named, rank.astype(jnp.int32), -1)
    slots = lax.broadcasted_iota(jnp.int32, (experts, capacity, tokens), 1)
    chosen = rank[:, None, :] == slots
    slot_weight = jnp.sum(jnp.where(chosen, weight[:, None, :], 0.0), axis=2)
    return chosen.reshape(experts * capacity, tokens).astype(BF16), slot_weight.reshape(-1, 1)


def body(
    chunks,
    cotangent,
    route_ids,
    route_weights,
    expert_inputs,
    gate_weight,
    up_weight,
    down_weight,
    out_weight,
    gate_in,
    conv_sum,
    conv_c,
    conv_v,
    conv_taps,
):
    groups = lax.axis_size("sp")
    lanes = lax.axis_size("tp")
    capacity = expert_inputs.shape[1] // groups
    experts = groups
    model_width = cotangent.shape[1]
    lane_cols = model_width // lanes
    own_rows = lax.dynamic_slice_in_dim(cotangent, lax.axis_index("tp") * lane_cols, lane_cols, 1)
    chosen, slot_weight = routing(route_ids, route_weights, experts, capacity)
    picked = jnp.dot(chosen, own_rows, preferred_element_type=F32)
    outgoing = (slot_weight * picked).astype(BF16)
    returned, grad_gate, grad_up, grad_down = run_experts(
        (groups, lanes, chunks, capacity),
        outgoing,
        expert_inputs[0],
        gate_weight[0],
        up_weight[0],
        down_weight[0],
    )
    returned_sum = lax.dot_general(
        chosen, returned, (((0,), (0,)), ((), ())), preferred_element_type=F32
    )
    grad_input = (own_rows.astype(F32) + returned_sum).astype(BF16)
    full_mid = collect(grad_input, "tp", 1)
    mixed_rows = (gate_in.astype(F32) * conv_sum.astype(F32)).astype(BF16)
    grad_mixed = jnp.dot(full_mid, out_weight, preferred_element_type=F32)
    grad_out_weight = summed_on_arrival(
        lax.dot_general(
            full_mid, mixed_rows, (((0,), (0,)), ((), ())), preferred_element_type=F32
        ),
        "sp",
        0,
    )
    grad_gate_in = (grad_mixed * conv_sum.astype(F32)).astype(BF16)
    grad_sum = grad_mixed * gate_in.astype(F32)
    next_rows = shifted(grad_sum[:2], "sp", -1)
    extended = jnp.concatenate([grad_sum, next_rows], axis=0)
    grad_prod = (
        conv_taps[0] * extended[2:] + conv_taps[1] * extended[1:-1] + conv_taps[2] * extended[:-2]
    )
    grad_conv_c = (grad_prod * conv_v.astype(F32)).astype(BF16)
    grad_conv_v = (grad_prod * conv_c.astype(F32)).astype(BF16)
    return (
        grad_input,
        grad_gate[None],
        grad_up[None],
        grad_down[None],
        grad_out_weight,
        grad_gate_in,
        grad_conv_c,
        grad_conv_v,
    )


def solution(mesh):
    placed = (
        P("sp", None),
        P("sp", None),
        P("sp", None),
        P("sp", None, None),
        P("sp", None, "tp"),
        P("sp", None, "tp"),
        P("sp", "tp", None),
        P(None, "tp"),
        P("sp", "tp"),
        P("sp", "tp"),
        P("sp", "tp"),
        P("sp", "tp"),
        P(None, "tp"),
    )
    chunks = min(8, mesh.shape["sp"] // 2)
    return jax.shard_map(
        functools.partial(body, chunks),
        mesh=mesh,
        in_specs=placed,
        out_specs=(
            P("sp", "tp"),
            P("sp", None, "tp"),
            P("sp", None, "tp"),
            P("sp", "tp", None),
            P("sp", "tp"),
            P("sp", "tp"),
            P("sp", "tp"),
            P("sp", "tp"),
        ),
        check_vma=False,
    )
```

time: 302 us -> 178 us (0.59)
  the two profiles are of different devices: /device:TPU:17 before, /device:TPU:1 now
where the time goes in v1:
time: 178 us; the launch traced here: 177 us
  Pallas kernels  108 us (61%)
  waiting for transfers between devices  23.2 us (13%)
  blocking collectives  20.9 us (12%)
  starting transfers between devices  8.82 us (5%)
  matrix products  6.81 us (4%)
  local copies, waits for them, and re-layouts  6.23 us (4%)
  other arithmetic  2.5 us (1%)
    pallas_call x1, Pallas kernels, run_experts(): pl.pallas_call(functools.partial(expert_kernel, dims), out_shape=(jax.Sha...  108 us
    all_to_all x1, blocking collectives, collect(): lax.all_to_all(copies, axis, split_axis=0, concat_axis=0, tiled=True)  20.9 us
    all_to_all x1, waiting for transfers between devices, summed_on_arrival(): lax.all_to_all(pieces, axis, split_axis=0, concat_axis=0, tiled=True)  20.4 us
    all_to_all x1, starting transfers between devices, summed_on_arrival(): lax.all_to_all(pieces, axis, split_axis=0, concat_axis=0, tiled=True)  6.34 us
    unnamed x21, local copies, waits for them, and re-layouts  4.34 us
  transfers between devices with their start and end apart: 2, of which 2 were waited for; matrix products, arithmetic and copies ran while one was open for 1% of the time, Pallas kernels for 0%

profile of v1, /device:TPU:1, one launch (start us, length us, event | category | flops | bytes accessed | tf_op | source)
XLA Modules:
  0.0 177.2 jit_solution(2507323895103146737)
XLA Ops:
  0.6 0.0 copy-start
  0.7 0.8 fusion.20
  1.4 0.8 fusion.19
  2.2 0.2 fusion.1
  2.4 0.2 select_reduce_fusion
  2.6 0.1 mul.59
  2.7 0.1 iota.37
  2.8 0.2 bitcast_compare_fusion
  3.0 2.4 %multiply_convert_fusion.out_ref = bf16[1024,512]{1,0:T(8,128)(2,1)} fusion(pred[1024,256]{1,0:T(32,128)(4,1)S(1)} %bitcast_compare_fusion, f32[1024]{0:T(1024)S(1)} %mul.59, bf16[256,2048]{1,0:T(8,128)(2,1)} %param.13, s32[]{:T(128)S(6)} %select_n.26), kind=kOutput, calls=%fused_computation | convolution fusion | flops 269484032 | bytes 1576964 | tf_op jit(solution)/shard_map/dot_general | solution.py:464
  5.4 108.0 %experts.1 = (bf16[1024,512]{1,0:T(8,128)(2,1)}, bf16[2048,256]{1,0:T(8,128)(2,1)}, bf16[2048,256]{1,0:T(8,128)(2,1)}, bf16[256,2048]{1,0:T(8,128)(2,1)}) custom-call(bf16[1024,512]{1,0:T(8,128)(2,1)} %multiply_convert_fusion.out_ref, bf16[1024,2048]{1,0:T(8,128)(2,1)} %bitcast.39, bf16[2048,256]{1,0:T(8,128)(2,1)} %bitcast.43, bf16[2048,256]{1,0:T(8,128)(2,1)} %bitcast.44, ...), custom_call_target="tpu_custom_call" | custom-call | tf_op jit(solution)/shard_map/experts/pallas_call | solution.py:376
  113.4 1.8 fusion
  115.1 0.0 copy-start.3
  115.1 0.0 copy-start.4
  115.2 0.0 copy-start.5
  115.2 0.1 copy.23
  115.3 0.1 broadcast_in_dim.63
  115.4 20.9 %all_to_all.10 = bf16[4,256,512]{1,2,0:T(8,128)(2,1)S(1)} all-to-all(bf16[4,256,512]{1,2,0:T(8,128)(2,1)S(1)} %broadcast_in_dim.63), channel_id=1, replica_groups=mesh['sp'=64,'tp'=4] {'tp'}, dimensions={0} | all-to-all | bytes 2097152 | tf_op jit(solution)/shard_map/all_to_all | solution.py:401
  136.3 0.0 copy-done.4
  136.3 0.0 copy-done.5
  136.3 1.4 fusion.11
  137.7 0.0 copy-done.3
  137.7 0.0 copy-start.8
  137.7 0.0 copy-start.6
  137.7 0.0 copy-start.7
  137.7 6.3 %all-to-all-start.1 = ((f32[64,32,128]{2,1,0:T(8,128)}), f32[64,32,128]{2,1,0:T(8,128)S(1)}, u32[]{:S(2)}, u32[]{:S(2)}) async-start(f32[64,32,128]{2,1,0:T(8,128)} %fusion.11), calls=%async_computation.1 | async-start | bytes 2097152 | tf_op jit(solution)/shard_map/all_to_all | solution.py:409
  144.1 0.0 copy-done
  144.1 1.1 convert_multiply_fusion.2
  145.2 0.0 copy-start.2
  145.2 2.5 %collective-permute-start = (f32[2,128]{1,0:T(2,128)S(1)}, f32[2,128]{1,0:T(2,128)S(1)}, u32[]{:S(2)}, u32[]{:S(2)}) collective-permute-start(f32[2,128]{1,0:T(2,128)S(1)} %slice.44), channel_id=1, source_target_pairs={{4,0},{8,4},{12,8},{16,12},{20,16},{24,20},{28,24},{32,28},{36,32}... | collective-permute-start | bytes 3080 | tf_op jit(solution)/shard_map/ppermute | solution.py:416
  147.7 0.0 copy-done.8
  147.7 2.8 %collective-permute-done = f32[2,128]{1,0:T(2,128)S(1)} collective-permute-done((f32[2,128]{1,0:T(2,128)S(1)}, f32[2,128]{1,0:T(2,128)S(1)}, u32[]{:S(2)}, u32[]{:S(2)}) %collective-permute-start) | collective-permute-done | bytes 1056 | tf_op jit(solution)/shard_map/ppermute | solution.py:416
  150.5 0.0 copy-done.6
  150.5 0.7 multiply_convert_fusion.1
  151.2 0.0 copy-done.7
  151.2 0.7 multiply_convert_fusion.2
  151.9 20.4 %all-to-all-done.1 = f32[64,32,128]{2,1,0:T(8,128)S(1)} async-done(((f32[64,32,128]{2,1,0:T(8,128)}), f32[64,32,128]{2,1,0:T(8,128)S(1)}, u32[]{:S(2)}, u32[]{:S(2)}) %all-to-all-start.1) | async-done | bytes 1048608 | tf_op jit(solution)/shard_map/all_to_all | solution.py:409
  172.2 0.7 reduce_sum.19
  172.9 0.0 copy-start.1
  172.9 2.4 %copy.30 = bf16[1,2048,256]{2,1,0:T(8,128)(2,1)} copy(bf16[1,2048,256]{2,1,0:T(8,128)(2,1)} %bitcast.42) | data formatting | bytes 2097152
  175.3 0.0 copy-done.2
  175.3 1.0 copy.31
  176.3 0.0 copy-done.1
  176.3 1.0 copy.32
  (4 shorter events, 0.0 us)
Async XLA Ops:
  0.6 143.4 %copy-start = (bf16[2048,128]{1,0:T(8,128)(2,1)S(1)}, bf16[2048,128]{1,0:T(8,128)(2,1)}, u32[]{:S(2)}) copy-start(bf16[2048,128]{1,0:T(8,128)(2,1)} %param.20) | copy-start | bytes 1572868
  115.1 22.6 %copy-start.3 = (bf16[256,512]{1,0:T(8,128)(2,1)}, bf16[256,512]{1,0:T(8,128)(2,1)S(1)}, u32[]{:S(2)}) copy-start(bf16[256,512]{1,0:T(8,128)(2,1)S(1)} %fusion) | copy-start | bytes 786436
  115.1 21.2 %copy-start.4 = (bf16[256,128]{1,0:T(8,128)(2,1)S(1)}, bf16[256,128]{1,0:T(8,128)(2,1)}, u32[]{:S(2)}) copy-start(bf16[256,128]{1,0:T(8,128)(2,1)} %param.22) | copy-start | bytes 196612
  115.2 21.2 %copy-start.5 = (bf16[256,128]{1,0:T(8,128)(2,1)S(1)}, bf16[256,128]{1,0:T(8,128)(2,1)}, u32[]{:S(2)}) copy-start(bf16[256,128]{1,0:T(8,128)(2,1)} %param.21) | copy-start | bytes 196612
  137.7 10.0 %copy-start.8 = (f32[3,128]{1,0:T(4,128)S(1)}, f32[3,128]{1,0:T(4,128)}, u32[]{:S(2)}) copy-start(f32[3,128]{1,0:T(4,128)} %param.25) | copy-start | bytes 4612
  137.7 12.8 %copy-start.6 = (bf16[256,128]{1,0:T(8,128)(2,1)S(1)}, bf16[256,128]{1,0:T(8,128)(2,1)}, u32[]{:S(2)}) copy-start(bf16[256,128]{1,0:T(8,128)(2,1)} %param.23) | copy-start | bytes 196612
  137.7 13.5 %copy-start.7 = (bf16[256,128]{1,0:T(8,128)(2,1)S(1)}, bf16[256,128]{1,0:T(8,128)(2,1)}, u32[]{:S(2)}) copy-start(bf16[256,128]{1,0:T(8,128)(2,1)} %param.24) | copy-start | bytes 196612
  137.7 34.5 %all-to-all-start.1 = ((f32[64,32,128]{2,1,0:T(8,128)}), f32[64,32,128]{2,1,0:T(8,128)S(1)}, u32[]{:S(2)}, u32[]{:S(2)}) async-start(f32[64,32,128]{2,1,0:T(8,128)} %fusion.11), calls=%async_computation.1 | async-start | bytes 2097152 | tf_op jit(solution)/shard_map/all_to_all | solution.py:409
  145.2 30.1 %copy-start.2 = (bf16[2048,256]{1,0:T(8,128)(2,1)S(1)}, bf16[2048,256]{1,0:T(8,128)(2,1)}, u32[]{:S(2)}) copy-start(bf16[2048,256]{1,0:T(8,128)(2,1)} %get-tuple-element.14) | copy-start | bytes 3145732
  145.2 5.3 %collective-permute-start = (f32[2,128]{1,0:T(2,128)S(1)}, f32[2,128]{1,0:T(2,128)S(1)}, u32[]{:S(2)}, u32[]{:S(2)}) collective-permute-start(f32[2,128]{1,0:T(2,128)S(1)} %slice.44), channel_id=1, source_target_pairs={{4,0},{8,4},{12,8},{16,12},{20,16},{24,20},{28,24},{32,28},{36,32}... | collective-permute-start | bytes 3080 | tf_op jit(solution)/shard_map/ppermute | solution.py:416
  172.9 3.3 %copy-start.1 = (bf16[256,2048]{1,0:T(8,128)(2,1)S(1)}, bf16[256,2048]{1,0:T(8,128)(2,1)}, u32[]{:S(2)}) copy-start(bf16[256,2048]{1,0:T(8,128)(2,1)} %get-tuple-element.15) | copy-start | bytes 3145732

commit v2 on v1

--- a/solution.py
+++ b/solution.py
@@ -13,17 +13,36 @@
 BF16 = jnp.bfloat16
 
 
-def expert_kernel(
+def step_kernel(
     dims,
     out_ref,
+    chosen,
+    own_rows,
+    out_weight,
+    gate_in,
+    conv_sum,
+    conv_c,
+    conv_v,
+    taps,
     x_hbm,
     gate_hbm,
     up_hbm,
     down_hbm,
-    returned,
+    grad_input,
     g_gate,
     g_up,
     g_down,
+    g_out,
+    g_gate_in,
+    g_conv_c,
+    g_conv_v,
+    returned,
+    chosen_t,
+    full_in,
+    mixed,
+    sums,
+    out_terms,
+    out_in,
     x_v,
     gate_v,
     up_v,
@@ -47,6 +66,12 @@
     recv_y,
     send_r,
     recv_r,
+    send_s,
+    recv_s,
+    send_o,
+    recv_o,
+    send_n,
+    recv_n,
 ):
     sps, tps, chunks, cap = dims
     group = sps // chunks
@@ -116,6 +141,9 @@
     lax.fori_loop(1, chunks, send_chunk, 0)
     own = pl.ds(pl.multiple_of(me * cap, cap), cap)
     routed[q, own, :] = out_ref[own, :]
+
+    chosen_t[...] = chosen[...].T
+    mixed[...] = (gate_in[...].astype(F32) * conv_sum[...].astype(F32)).astype(BF16)
 
     for load in loads:
         load.wait()
@@ -278,7 +306,7 @@
     stages = (stage_gather, stage_pass, stage_compute, stage_first, stage_return)
 
     def step(t, carry):
-        for depth, stage in reversed(tuple(enumerate(stages))):
+        for depth, stage in enumerate(stages):
             i = t - depth
 
             @pl.when((i >= 0) & (i < chunks))
@@ -289,8 +317,80 @@
 
     lax.fori_loop(0, chunks + len(stages) - 1, step, 0)
     returned[own, :] = ret_src[own, :]
+    rest = pl.ds(0, (sps - 1) * cap)
+    final = pltpu.make_async_remote_copy(
+        src_ref=ret_src.at[rest, :],
+        dst_ref=returned.at[rest, :],
+        send_sem=send_r,
+        recv_sem=recv_r,
+        device_id=(me, up_q),
+        device_id_type=MESH,
+    )
+    final.wait_recv()
+
+    tokens = grad_input.shape[0]
+    own_grad = (
+        own_rows[...].astype(F32)
+        + jnp.dot(chosen_t[...], returned[...], preferred_element_type=F32)
+    ).astype(BF16)
+    grad_input[...] = own_grad
+    full_in[q] = own_grad
+
+    def share(lane, first, size, kind, peer):
+        ref = full_in.at[lane, pl.ds(first, size), :]
+        return pltpu.make_async_remote_copy(
+            src_ref=ref,
+            dst_ref=ref,
+            send_sem=send_s.at[kind],
+            recv_sem=recv_s.at[kind],
+            device_id=(me, peer),
+            device_id_type=MESH,
+        )
+
+    split = tokens // 2
+    shares = (
+        share(q, 0, tokens, 0, up_q),
+        share(q, 0, tokens, 1, dn_q),
+        share(dn_q, 0, split, 2, up_q),
+        share(up_q, split, split, 3, dn_q),
+    )
+    shares[0].start()
+    shares[1].start()
 
     contract0 = (((0,), (0,)), ((), ()))
+    per_lane = sps // tps
+    owned = g_out.shape[0]
+
+    def send_terms(lane):
+        out_terms[lane] = lax.dot_general(
+            full_in[lane], mixed[...], contract0, preferred_element_type=F32
+        ).astype(BF16)
+
+        def send_one(k, carry):
+            place = (g + k) % per_lane
+            owner = lane * per_lane + place
+
+            @pl.when(owner != me)
+            def _():
+                pltpu.make_async_remote_copy(
+                    src_ref=out_terms.at[lane, pl.ds(pl.multiple_of(place * owned, owned), owned), :],
+                    dst_ref=out_in.at[me],
+                    send_sem=send_o,
+                    recv_sem=recv_o,
+                    device_id=(owner, q),
+                    device_id_type=MESH,
+                ).start()
+
+            @pl.when(owner == me)
+            def _():
+                out_in[me] = out_terms[lane, pl.ds(pl.multiple_of(place * owned, owned), owned), :]
+
+            return carry
+
+        lax.fori_loop(0, per_lane, send_one, 0)
+
+    send_terms(q)
+
     for lane in range(tps):
         span = slice(lane * cols, (lane + 1) * cols)
         g_down[:, span] = lax.dot_general(
@@ -303,6 +403,66 @@
             x_v[:, span], gpu_s[...], contract0, preferred_element_type=F32
         ).astype(BF16)
 
+    shares[0].wait_recv()
+    shares[2].start()
+    shares[1].wait_recv()
+    shares[3].start()
+    send_terms(dn_q)
+    send_terms(up_q)
+    shares[2].wait_recv()
+    shares[3].wait_recv()
+    send_terms(far_q)
+
+    grad_mixed = jnp.zeros((tokens, out_weight.shape[1]), F32)
+    for lane in range(tps):
+        grad_mixed += jnp.dot(
+            full_in[lane],
+            out_weight[lane * cols : (lane + 1) * cols, :],
+            preferred_element_type=F32,
+        )
+    sums[0:tokens, :] = grad_mixed * gate_in[...].astype(F32)
+    edge = sums.shape[0] - tokens
+    shift = pltpu.make_async_remote_copy(
+        src_ref=sums.at[pl.ds(0, edge), :],
+        dst_ref=sums.at[pl.ds(tokens, edge), :],
+        send_sem=send_n,
+        recv_sem=recv_n,
+        device_id=((me + sps - 1) % sps, q),
+        device_id_type=MESH,
+    )
+    shift.start()
+    g_gate_in[...] = (grad_mixed * conv_sum[...].astype(F32)).astype(BF16)
+    shift.wait_recv()
+
+    @pl.when(me == sps - 1)
+    def _():
+        sums[tokens : tokens + edge, :] = jnp.zeros((edge, sums.shape[1]), F32)
+
+    grad_prod = (
+        taps[0:1, :] * sums[2 : tokens + 2, :]
+        + taps[1:2, :] * sums[1 : tokens + 1, :]
+        + taps[2:3, :] * sums[0:tokens, :]
+    )
+    g_conv_c[...] = (grad_prod * conv_v[...].astype(F32)).astype(BF16)
+    g_conv_v[...] = (grad_prod * conv_c[...].astype(F32)).astype(BF16)
+
+    others = out_in.at[pl.ds(0, sps - 1)]
+    terms = pltpu.make_async_remote_copy(
+        src_ref=others,
+        dst_ref=others,
+        send_sem=send_o,
+        recv_sem=recv_o,
+        device_id=(me, up_q),
+        device_id_type=MESH,
+    )
+    terms.wait_recv()
+    g_out[...] = jnp.sum(out_in[...].astype(F32), axis=0)
+
+    terms.wait_send()
+    shift.wait_send()
+    for copy in shares:
+        copy.wait_send()
+
     def drain(i, carry):
         for copy in every:
             copy(i).wait_send()
@@ -328,27 +488,29 @@
         return carry
 
     lax.fori_loop(1, chunks, drain_rest, 0)
-    rest = pl.ds(0, (sps - 1) * cap)
-    final = pltpu.make_async_remote_copy(
-        src_ref=ret_src.at[rest, :],
-        dst_ref=returned.at[rest, :],
-        send_sem=send_r,
-        recv_sem=recv_r,
-        device_id=(me, up_q),
-        device_id_type=MESH,
-    )
     final.wait_send()
-    final.wait_recv()
-
-
-def run_experts(dims, outgoing, x, gate, up, down):
+
+
+def run_step(dims, small, large):
     sps, tps, chunks, cap = dims
+    outgoing, chosen, own_rows, out_weight = small[:4]
+    gate = large[1]
     rows, cols = outgoing.shape
+    tokens = own_rows.shape[0]
+    lane_w = out_weight.shape[1]
     width, units = gate.shape
     rows_c = rows // chunks
     vmem = pl.BlockSpec(memory_space=pltpu.VMEM)
     hbm = pl.BlockSpec(memory_space=pltpu.HBM)
+    dma = pltpu.SemaphoreType.DMA
     scratch = [
+        pltpu.VMEM((rows, cols), BF16),
+        pltpu.VMEM((tokens, rows), BF16),
+        pltpu.VMEM((tps, tokens, cols), BF16),
+        pltpu.VMEM((tokens, lane_w), BF16),
+        pltpu.VMEM((tokens + 8, lane_w), F32),
+        pltpu.VMEM((tps, cols, lane_w), BF16),
+        pltpu.VMEM((sps, width // sps, lane_w), BF16),
         pltpu.VMEM((rows, width), BF16),
         pltpu.VMEM((width, units), BF16),
         pltpu.VMEM((width, units), BF16),
@@ -365,55 +527,41 @@
         pltpu.VMEM((rows, units), BF16),
         pltpu.VMEM((rows, units), BF16),
         pltpu.VMEM((rows, units), BF16),
-        pltpu.SemaphoreType.DMA((4,)),
-        pltpu.SemaphoreType.DMA((chunks,)),
-        pltpu.SemaphoreType.DMA((chunks,)),
-        pltpu.SemaphoreType.DMA((8, chunks)),
-        pltpu.SemaphoreType.DMA((8, chunks)),
-        pltpu.SemaphoreType.DMA,
-        pltpu.SemaphoreType.DMA,
+        dma((4,)),
+        dma((chunks,)),
+        dma((chunks,)),
+        dma((8, chunks)),
+        dma((8, chunks)),
+        dma,
+        dma,
+        dma((4,)),
+        dma((4,)),
+        dma,
+        dma,
+        dma,
+        dma,
     ]
+    outs = (
+        ((tokens, cols), BF16),
+        ((width, units), BF16),
+        ((width, units), BF16),
+        ((units, width), BF16),
+        ((width // sps, lane_w), F32),
+        ((tokens, lane_w), BF16),
+        ((tokens, lane_w), BF16),
+        ((tokens, lane_w), BF16),
+    )
     return pl.pallas_call(
-        functools.partial(expert_kernel, dims),
-        out_shape=(
-            jax.ShapeDtypeStruct((rows, cols), BF16),
-            jax.ShapeDtypeStruct((width, units), BF16),
-            jax.ShapeDtypeStruct((width, units), BF16),
-            jax.ShapeDtypeStruct((units, width), BF16),
-        ),
-        in_specs=[vmem, hbm, hbm, hbm, hbm],
-        out_specs=(vmem, vmem, vmem, vmem),
+        functools.partial(step_kernel, dims),
+        out_shape=tuple(jax.ShapeDtypeStruct(*out) for out in outs),
+        in_specs=[vmem] * len(small) + [hbm] * len(large),
+        out_specs=(vmem,) * len(outs),
         scratch_shapes=scratch,
         compiler_params=pltpu.CompilerParams(
             collective_id=0, has_side_effects=True, vmem_limit_bytes=60 * 1024 * 1024
         ),
-        name="experts",
-    )(outgoing, x, gate, up, down)
-
-
-def split_up(value, dim, peers):
-    before, after = (value.shape[:dim], value.shape[dim + 1 :])
-    return jnp.moveaxis(value.reshape(*before, peers, -1, *after), dim, 0)
-
-
-def collect(value, axis, dim):
-    copies = jnp.broadcast_to(value, (lax.axis_size(axis), *value.shape))
-    pieces = lax.all_to_all(copies, axis, split_axis=0, concat_axis=0, tiled=True)
-    shape = list(value.shape)
-    shape[dim] *= pieces.shape[0]
-    return jnp.moveaxis(pieces, 0, dim).reshape(shape)
-
-
-def summed_on_arrival(value, axis, dim):
-    pieces = split_up(value, dim, lax.axis_size(axis))
-    arrived = lax.all_to_all(pieces, axis, split_axis=0, concat_axis=0, tiled=True)
-    return arrived.astype(F32).sum(axis=0)
-
-
-def shifted(block, axis, distance):
-    devices = range(lax.axis_size(axis))
-    route = [(i - distance, i) for i in devices if i - distance in devices]
-    return lax.ppermute(block, axis, route)
+        name="step",
+    )(*small, *large)
 
 
 def routing(route_ids, route_weights, experts, capacity):
@@ -463,47 +611,22 @@
     chosen, slot_weight = routing(route_ids, route_weights, experts, capacity)
     picked = jnp.dot(chosen, own_rows, preferred_element_type=F32)
     outgoing = (slot_weight * picked).astype(BF16)
-    returned, grad_gate, grad_up, grad_down = run_experts(
+    grad_input, grad_gate, grad_up, grad_down, *rest = run_step(
         (groups, lanes, chunks, capacity),
-        outgoing,
-        expert_inputs[0],
-        gate_weight[0],
-        up_weight[0],
-        down_weight[0],
-    )
-    returned_sum = lax.dot_general(
-        chosen, returned, (((0,), (0,)), ((), ())), preferred_element_type=F32
-    )
-    grad_input = (own_rows.astype(F32) + returned_sum).astype(BF16)
-    full_mid = collect(grad_input, "tp", 1)
-    mixed_rows = (gate_in.astype(F32) * conv_sum.astype(F32)).astype(BF16)
-    grad_mixed = jnp.dot(full_mid, out_weight, preferred_element_type=F32)
-    grad_out_weight = summed_on_arrival(
-        lax.dot_general(
-            full_mid, mixed_rows, (((0,), (0,)), ((), ())), preferred_element_type=F32
+        (
+            outgoing,
+            chosen,
+            own_rows,
+            out_weight,
+            gate_in,
+            conv_sum,
+            conv_c,
+            conv_v,
+            conv_taps,
         ),
-        "sp",
-        0,
-    )
-    grad_gate_in = (grad_mixed * conv_sum.astype(F32)).astype(BF16)
-    grad_sum = grad_mixed * gate_in.astype(F32)
-    next_rows = shifted(grad_sum[:2], "sp", -1)
-    extended = jnp.concatenate([grad_sum, next_rows], axis=0)
-    grad_prod = (
-        conv_taps[0] * extended[2:] + conv_taps[1] * extended[1:-1] + conv_taps[2] * extended[:-2]
-    )
-    grad_conv_c = (grad_prod * conv_v.astype(F32)).astype(BF16)
-    grad_conv_v = (grad_prod * conv_c.astype(F32)).astype(BF16)
-    return (
-        grad_input,
-        grad_gate[None],
-        grad_up[None],
-        grad_down[None],
-        grad_out_weight,
-        grad_gate_in,
-        grad_conv_c,
-        grad_conv_v,
-    )
+        (expert_inputs[0], gate_weight[0], up_weight[0], down_weight[0]),
+    )
+    return (grad_input, grad_gate[None], grad_up[None], grad_down[None], *rest)
 
 
 def solution(mesh):

time: 178 us -> 145 us (0.81)
  the two profiles are of different devices: /device:TPU:1 before, /device:TPU:17 now
where the time goes in v2:
time: 145 us; the launch traced here: 144 us
  Pallas kernels  130 us (90%)
  local copies, waits for them, and re-layouts  10.3 us (7%)
  matrix products  1.58 us (1%)
    pallas_call x1, Pallas kernels, run_step(): pl.pallas_call(functools.partial(step_kernel, dims), out_shape=tuple((jax...  130 us
    unnamed x24, local copies, waits for them, and re-layouts  8.58 us

profile of v2, /device:TPU:17, one launch (start us, length us, event | category | flops | bytes accessed | tf_op | source)
XLA Modules:
  0.0 144.3 jit_solution(2450900970868686568)
XLA Ops:
  0.6 0.0 copy-start
  0.7 0.8 fusion.7
  1.4 0.8 fusion.6
  2.2 0.1 iota.38
  2.3 0.2 fusion
  2.5 0.2 select_reduce_fusion
  2.7 0.1 mul.13
  2.8 0.0 copy-done
  2.8 0.0 copy-start.1
  2.8 1.1 fusion.5
  3.9 1.4 multiply_convert_fusion.out_ref
  5.3 0.0 copy-done.1
  5.3 130.5 %step.1 = (bf16[256,512]{1,0:T(8,128)(2,1)}, bf16[2048,256]{1,0:T(8,128)(2,1)}, bf16[2048,256]{1,0:T(8,128)(2,1)}, bf16[256,2048]{1,0:T(8,128)(2,1)}, f32[32,128...) custom-call(bf16[1024,512]{1,0:T(8,128)(2,1)} %multiply_convert_fusion.out_ref, ...), custom_call_target="tpu_custom_call" | custom-call | tf_op jit(solution)/shard_map/step/pallas_call | solution.py:554
  135.7 0.0 copy-start.3
  135.8 1.8 %copy.31 = bf16[256,512]{1,0:T(8,128)(2,1)} copy(bf16[256,512]{1,0:T(8,128)(2,1)} %get-tuple-element.38) | data formatting | bytes 524288
  137.5 0.0 copy-start.2
  137.5 2.4 %copy.32 = bf16[1,2048,256]{2,1,0:T(8,128)(2,1)} copy(bf16[1,2048,256]{2,1,0:T(8,128)(2,1)} %bitcast.22) | data formatting | bytes 2097152
  139.9 0.0 copy-done.3
  139.9 0.0 copy-start.7
  139.9 0.0 copy-start.6
  139.9 0.0 copy-start.5
  139.9 0.0 copy-start.4
  139.9 1.0 copy.33
  140.9 0.0 copy-done.2
  140.9 1.0 copy.34
  141.8 0.0 copy-done.7
  141.8 0.6 copy.35
  142.4 0.0 copy-done.6
  142.4 0.6 copy.36
  143.1 0.0 copy-done.5
  143.1 0.6 copy.37
  143.7 0.0 copy-done.4
  143.7 0.6 copy.38
  (3 shorter events, 0.0 us)
Async XLA Ops:
  0.6 2.1 %copy-start = (bf16[256,2048]{1,0:T(8,128)(2,1)S(1)}, bf16[256,2048]{1,0:T(8,128)(2,1)}, u32[]{:S(2)}) copy-start(bf16[256,2048]{1,0:T(8,128)(2,1)} %param.13) | copy-start | bytes 3145732
  2.8 2.5 %copy-start.1 = (bf16[256,512]{1,0:T(8,128)(2,1)}, bf16[256,512]{1,0:T(8,128)(2,1)S(1)}, u32[]{:S(2)}) copy-start(bf16[256,512]{1,0:T(8,128)(2,1)S(1)} %constant_dynamic-slice_fusion.own_rows) | copy-start | bytes 786436
  135.7 4.1 %copy-start.3 = (bf16[2048,256]{1,0:T(8,128)(2,1)S(1)}, bf16[2048,256]{1,0:T(8,128)(2,1)}, u32[]{:S(2)}) copy-start(bf16[2048,256]{1,0:T(8,128)(2,1)} %get-tuple-element.18) | copy-start | bytes 3145732
  137.5 3.4 %copy-start.2 = (bf16[256,2048]{1,0:T(8,128)(2,1)S(1)}, bf16[256,2048]{1,0:T(8,128)(2,1)}, u32[]{:S(2)}) copy-start(bf16[256,2048]{1,0:T(8,128)(2,1)} %get-tuple-element.19) | copy-start | bytes 3145732
  139.9 2.0 %copy-start.7 = (f32[32,128]{1,0:T(8,128)S(1)}, f32[32,128]{1,0:T(8,128)}, u32[]{:S(2)}) copy-start(f32[32,128]{1,0:T(8,128)} %get-tuple-element.42) | copy-start | bytes 49156
  139.9 2.6 %copy-start.6 = (bf16[256,128]{1,0:T(8,128)(2,1)S(1)}, bf16[256,128]{1,0:T(8,128)(2,1)}, u32[]{:S(2)}) copy-start(bf16[256,128]{1,0:T(8,128)(2,1)} %get-tuple-element.43) | copy-start | bytes 196612
  139.9 3.2 %copy-start.5 = (bf16[256,128]{1,0:T(8,128)(2,1)S(1)}, bf16[256,128]{1,0:T(8,128)(2,1)}, u32[]{:S(2)}) copy-start(bf16[256,128]{1,0:T(8,128)(2,1)} %get-tuple-element.44) | copy-start | bytes 196612
  139.9 3.8 %copy-start.4 = (bf16[256,128]{1,0:T(8,128)(2,1)S(1)}, bf16[256,128]{1,0:T(8,128)(2,1)}, u32[]{:S(2)}) copy-start(bf16[256,128]{1,0:T(8,128)(2,1)} %get-tuple-element.45) | copy-start | bytes 196612

commit v3 on v2

--- a/solution.py
+++ b/solution.py
@@ -7,7 +7,6 @@
 from jax.experimental.pallas import tpu as pltpu
 from jax.sharding import PartitionSpec as P
 
-TOP = 2
 MESH = pl.DeviceIdType.MESH
 F32 = jnp.float32
 BF16 = jnp.bfloat16
@@ -15,9 +14,9 @@
 
 def step_kernel(
     dims,
-    out_ref,
-    chosen,
-    own_rows,
+    ids,
+    weights,
+    cot,
     out_weight,
     gate_in,
     conv_sum,
@@ -36,6 +35,10 @@
     g_gate_in,
     g_conv_c,
     g_conv_v,
+    out_ref,
+    near_ref,
+    chosen,
+    slot_weight,
     returned,
     chosen_t,
     full_in,
@@ -74,10 +77,13 @@
     recv_n,
 ):
     sps, tps, chunks, cap = dims
+    near = 3
     group = sps // chunks
     rows_c = group * cap
     half = rows_c // 2
     cols = out_ref.shape[1]
+    tokens = cot.shape[0]
+    rows_all = sps * cap
     me = lax.axis_index("sp")
     q = lax.axis_index("tp")
     z = me // group
@@ -106,51 +112,111 @@
     lax.fori_loop(1, sps, greet, 0)
     for peer in (up_q, dn_q):
         pl.semaphore_signal(barrier, inc=1, device_id=(me, peer), device_id_type=MESH)
+
+    names = lax.broadcasted_iota(jnp.int32, (sps, tokens), 0)
+    first, second = names == ids[0:1, :], names == ids[1:2, :]
+    weight = jnp.where(first, weights[0:1, :], 0.0) + jnp.where(second, weights[1:2, :], 0.0)
+    named = first | second
+    earlier = lax.broadcasted_iota(jnp.int32, (tokens, tokens), 0) < lax.broadcasted_iota(
+        jnp.int32, (tokens, tokens), 1
+    )
+    rank = jnp.dot(
+        jnp.where(named, 1.0, 0.0).astype(BF16),
+        jnp.where(earlier, 1.0, 0.0).astype(BF16),
+        preferred_element_type=F32,
+    ).astype(jnp.int32)
+    rank = jnp.where(named, rank, -1)
+    pick = rank[:, None, :] == lax.broadcasted_iota(jnp.int32, (sps, cap, tokens), 1)
+    chosen[...] = jnp.where(pick, 1.0, 0.0).reshape(rows_all, tokens).astype(BF16)
+    slot_weight[...] = jnp.sum(
+        jnp.where(pick, weight[:, None, :], 0.0).reshape(rows_all, tokens), axis=1, keepdims=True
+    )
+    lane_span = pl.ds(pl.multiple_of(q * cols, cols), cols)
+    for slot, step_z in enumerate((0, 1, chunks - 1)):
+        rows = pl.ds(pl.multiple_of(((z + step_z) % chunks) * rows_c, rows_c), rows_c)
+        near_ref[slot * rows_c : (slot + 1) * rows_c, :] = (
+            slot_weight[rows, :]
+            * jnp.dot(chosen[rows, :], cot[...], preferred_element_type=F32)
+        ).astype(BF16)
+    out_ref[...] = (
+        slot_weight[...] * jnp.dot(chosen[...], cot[:, lane_span], preferred_element_type=F32)
+    ).astype(BF16)
     pl.semaphore_wait(barrier, sps - 1 + 2)
 
+    far_last = chunks - near
+
     def offset(i):
-        return ((i + 1) // 2) * (2 * (i % 2) - 1)
+        u = (i + chunks - 1) % chunks
+        w = u // (chunks - 3)
+        far = (2 + u // 2) * (1 - 2 * (u % 2))
+        return ((i + chunks - 1) // chunks) * (
+            (1 - w) * far + w * (1 - 2 * ((u - (chunks - 3)) % 2))
+        )
 
     def chunk_start(i):
         return ((z - offset(i) + chunks) % chunks) * rows_c
 
-    def block_copy(i, k):
-        peer = ((z + offset(i) + chunks) % chunks) * group + (g + k) % group
+    def peer_of(i, k):
+        return ((z + offset(i) + chunks) % chunks) * group + (g + k) % group
+
+    own = pl.ds(pl.multiple_of(me * cap, cap), cap)
+
+    def near_copy(i, slot, k):
+        row = slot * rows_c + ((g + k) % group) * cap
+        return pltpu.make_async_remote_copy(
+            src_ref=near_ref.at[pl.ds(pl.multiple_of(row, cap), cap), :],
+            dst_ref=routed.at[own, :],
+            send_sem=send_z.at[i],
+            recv_sem=recv_z.at[i],
+            device_id=(peer_of(i, k), q),
+            device_id_type=MESH,
+        )
+
+    def far_copy(i, k):
+        peer = peer_of(i, k)
         return pltpu.make_async_remote_copy(
             src_ref=out_ref.at[pl.ds(pl.multiple_of(peer * cap, cap), cap), :],
-            dst_ref=routed.at[q, pl.ds(pl.multiple_of(me * cap, cap), cap), :],
+            dst_ref=routed.at[own, lane_span],
             send_sem=send_z.at[i],
             recv_sem=recv_z.at[i],
             device_id=(peer, q),
             device_id_type=MESH,
         )
 
-    def send_first(k, carry):
-        block_copy(0, k).start()
+    def send_own(k, carry):
+        near_copy(0, 0, k).start()
         return carry
 
-    lax.fori_loop(1, group, send_first, 0)
-
-    def send_chunk(i, carry):
+    def send_far(i, carry):
         def send_one(k, inner):
-            block_copy(i, k).start()
+            far_copy(i, k).start()
             return inner
 
         return lax.fori_loop(0, group, send_one, carry)
 
-    lax.fori_loop(1, chunks, send_chunk, 0)
-    own = pl.ds(pl.multiple_of(me * cap, cap), cap)
-    routed[q, own, :] = out_ref[own, :]
+    def send_near(i, carry):
+        def send_one(k, inner):
+            near_copy(i, i - far_last, k).start()
+            return inner
+
+        return lax.fori_loop(0, group, send_one, carry)
+
+    lax.fori_loop(1, group, send_own, 0)
+    lax.fori_loop(1, far_last + 1, send_far, 0)
+    lax.fori_loop(far_last + 1, chunks, send_near, 0)
+    routed[own, :] = near_ref[pl.ds(pl.multiple_of(g * cap, cap), cap), :]
 
     chosen_t[...] = chosen[...].T
     mixed[...] = (gate_in[...].astype(F32) * conv_sum[...].astype(F32)).astype(BF16)
 
     for load in loads:
         load.wait()
-    pre_rows = 2 * rows_c
-
-    def forward(b, carry):
-        rows = pl.ds(pl.multiple_of(b * pre_rows, pre_rows), pre_rows)
+
+    def at(i, first=0, size=None):
+        return pl.ds(pl.multiple_of(chunk_start(i) + first, half), size or rows_c)
+
+    def forward(i):
+        rows = at(i)
         pre_gate = jnp.dot(x_v[rows, :], gate_v[...], preferred_element_type=F32)
         pre_up = jnp.dot(x_v[rows, :], up_v[...], preferred_element_type=F32)
         sig = jax.nn.sigmoid(pre_gate)
@@ -158,12 +224,6 @@
         swish_s[rows, :] = swish
         slope_s[rows, :] = pre_up * sig * (1.0 + pre_gate * (1.0 - sig))
         hidden_s[rows, :] = (swish * pre_up).astype(BF16)
-        return carry
-
-    lax.fori_loop(0, sps * cap // pre_rows, forward, 0)
-
-    def at(i, first=0, size=None):
-        return pl.ds(pl.multiple_of(chunk_start(i) + first, half), size or rows_c)
 
     def y_copy(src, dst, kind, i, peer):
         return pltpu.make_async_remote_copy(
@@ -175,20 +235,23 @@
             device_id_type=MESH,
         )
 
+    def lanes_of(lane):
+        return pl.ds(pl.multiple_of(lane * cols, cols), cols)
+
     def gather_up(i):
-        ref = routed.at[q, at(i), :]
+        ref = routed.at[at(i), lanes_of(q)]
         return y_copy(ref, ref, 0, i, up_q)
 
     def gather_dn(i):
-        ref = routed.at[q, at(i), :]
+        ref = routed.at[at(i), lanes_of(q)]
         return y_copy(ref, ref, 1, i, dn_q)
 
     def pass_up(i):
-        ref = routed.at[dn_q, at(i, 0, half), :]
+        ref = routed.at[at(i, 0, half), lanes_of(dn_q)]
         return y_copy(ref, ref, 2, i, up_q)
 
     def pass_dn(i):
-        ref = routed.at[up_q, at(i, half, half), :]
+        ref = routed.at[at(i, half, half), lanes_of(up_q)]
         return y_copy(ref, ref, 3, i, dn_q)
 
     def first_up(i):
@@ -205,26 +268,29 @@
 
     every = (gather_up, gather_dn, pass_up, pass_dn, first_up, first_dn, last_up, last_dn)
 
-    def wait_z(i, count):
-        rows = pl.ds(0, count * cap)
-        pltpu.make_async_remote_copy(
-            src_ref=out_ref.at[rows, :],
-            dst_ref=routed.at[q, rows, :],
+    def far_block(i):
+        return pltpu.make_async_remote_copy(
+            src_ref=out_ref.at[pl.ds(0, rows_c), :],
+            dst_ref=routed.at[pl.ds(0, rows_c), lane_span],
             send_sem=send_z.at[i],
             recv_sem=recv_z.at[i],
             device_id=(me, up_q),
             device_id_type=MESH,
-        ).wait_recv()
+        )
+
+    def near_block(i, count):
+        rows = pl.ds(0, count * cap)
+        return pltpu.make_async_remote_copy(
+            src_ref=near_ref.at[rows, :],
+            dst_ref=routed.at[rows, :],
+            send_sem=send_z.at[i],
+            recv_sem=recv_z.at[i],
+            device_id=(me, up_q),
+            device_id_type=MESH,
+        )
 
     def stage_gather(i):
-        @pl.when(i == 0)
-        def _():
-            wait_z(i, group - 1)
-
-        @pl.when(i > 0)
-        def _():
-            wait_z(i, group)
-
+        far_block(i).wait_recv()
         gather_up(i).start()
         gather_dn(i).start()
 
@@ -234,14 +300,12 @@
         gather_dn(i).wait_recv()
         pass_dn(i).start()
 
-    def stage_compute(i):
-        pass_up(i).wait_recv()
-        pass_dn(i).wait_recv()
+    def compute(i):
         rows = at(i)
         grad_hidden = jnp.zeros((rows_c, down_v.shape[0]), F32)
         for lane in range(tps):
             grad_hidden += lax.dot_general(
-                routed[lane, rows, :],
+                routed[rows, lane * cols : (lane + 1) * cols],
                 down_v[:, lane * cols : (lane + 1) * cols],
                 (((1,), (1,)), ((), ())),
                 preferred_element_type=F32,
@@ -262,6 +326,18 @@
         first_up(i).start()
         first_dn(i).start()
 
+    def stage_compute(i):
+        @pl.when(i <= far_last)
+        def _():
+            pass_up(i).wait_recv()
+            pass_dn(i).wait_recv()
+
+        @pl.when(i > far_last)
+        def _():
+            near_block(i, group).wait_recv()
+
+        compute(i)
+
     def stage_first(i):
         lower, upper = at(i, 0, half), at(i, half, half)
         first_up(i).wait_recv()
@@ -303,19 +379,31 @@
 
         lax.fori_loop(1, group, send_one, 0)
 
-    stages = (stage_gather, stage_pass, stage_compute, stage_first, stage_return)
+    forward(0)
+    if group > 1:
+        near_block(0, group - 1).wait_recv()
+    compute(0)
+    forward(1)
+    stage_first(0)
 
     def step(t, carry):
-        for depth, stage in enumerate(stages):
-            i = t - depth
-
-            @pl.when((i >= 0) & (i < chunks))
+        for stage, lead, first, last in (
+            (stage_gather, 1, 1, far_last),
+            (stage_pass, 0, 1, far_last),
+            (stage_compute, -1, 1, chunks - 1),
+            (forward, 2, 2, chunks - 1),
+            (stage_first, -2, 1, chunks - 1),
+            (stage_return, -3, 0, chunks - 1),
+        ):
+            i = t + lead
+
+            @pl.when((i >= first) & (i <= last))
             def _():
                 stage(i)
 
         return carry
 
-    lax.fori_loop(0, chunks + len(stages) - 1, step, 0)
+    lax.fori_loop(0, chunks + 3, step, 0)
     returned[own, :] = ret_src[own, :]
     rest = pl.ds(0, (sps - 1) * cap)
     final = pltpu.make_async_remote_copy(
@@ -328,9 +416,8 @@
     )
     final.wait_recv()
 
-    tokens = grad_input.shape[0]
     own_grad = (
-        own_rows[...].astype(F32)
+        cot[:, lane_span].astype(F32)
         + jnp.dot(chosen_t[...], returned[...], preferred_element_type=F32)
     ).astype(BF16)
     grad_input[...] = own_grad
@@ -394,7 +481,7 @@
     for lane in range(tps):
         span = slice(lane * cols, (lane + 1) * cols)
         g_down[:, span] = lax.dot_general(
-            hidden_s[...], routed[lane], contract0, preferred_element_type=F32
+            hidden_s[...], routed[:, span], contract0, preferred_element_type=F32
         ).astype(BF16)
         g_gate[span, :] = lax.dot_general(
             x_v[:, span], gpg_s[...], contract0, preferred_element_type=F32
@@ -463,40 +550,36 @@
     for copy in shares:
         copy.wait_send()
 
-    def drain(i, carry):
-        for copy in every:
+    def drain_far(i, carry):
+        for copy in every[:4]:
+            copy(i).wait_send()
+        far_block(i).wait_send()
+        return carry
+
+    def drain_sum(i, carry):
+        for copy in every[4:]:
             copy(i).wait_send()
         return carry
 
-    lax.fori_loop(0, chunks, drain, 0)
-
-    def drain_z(i, count):
-        rows = pl.ds(0, count * cap)
-        pltpu.make_async_remote_copy(
-            src_ref=out_ref.at[rows, :],
-            dst_ref=routed.at[q, rows, :],
-            send_sem=send_z.at[i],
-            recv_sem=recv_z.at[i],
-            device_id=(me, up_q),
-            device_id_type=MESH,
-        ).wait_send()
-
-    drain_z(0, group - 1)
-
-    def drain_rest(i, carry):
-        drain_z(i, group)
+    def drain_near(i, carry):
+        near_block(i, group).wait_send()
         return carry
 
-    lax.fori_loop(1, chunks, drain_rest, 0)
+    lax.fori_loop(1, far_last + 1, drain_far, 0)
+    lax.fori_loop(0, chunks, drain_sum, 0)
+    lax.fori_loop(far_last + 1, chunks, drain_near, 0)
+    if group > 1:
+        near_block(0, group - 1).wait_send()
     final.wait_send()
 
 
 def run_step(dims, small, large):
     sps, tps, chunks, cap = dims
-    outgoing, chosen, own_rows, out_weight = small[:4]
+    cot, out_weight = small[2:4]
     gate = large[1]
-    rows, cols = outgoing.shape
-    tokens = own_rows.shape[0]
+    rows = sps * cap
+    tokens = cot.shape[0]
+    cols = cot.shape[1] // tps
     lane_w = out_weight.shape[1]
     width, units = gate.shape
     rows_c = rows // chunks
@@ -504,6 +587,10 @@
     hbm = pl.BlockSpec(memory_space=pltpu.HBM)
     dma = pltpu.SemaphoreType.DMA
     scratch = [
+        pltpu.VMEM((rows, cols), BF16),
+        pltpu.VMEM((3 * rows_c, width), BF16),
+        pltpu.VMEM((rows, tokens), BF16),
+        pltpu.VMEM((rows, 1), F32),
         pltpu.VMEM((rows, cols), BF16),
         pltpu.VMEM((tokens, rows), BF16),
         pltpu.VMEM((tps, tokens, cols), BF16),
@@ -515,7 +602,7 @@
         pltpu.VMEM((width, units), BF16),
         pltpu.VMEM((width, units), BF16),
         pltpu.VMEM((units, width), BF16),
-        pltpu.VMEM((tps, rows, cols), BF16),
+        pltpu.VMEM((rows, width), BF16),
         pltpu.VMEM((tps, rows, cols), BF16),
         pltpu.VMEM((chunks, rows_c // 2, cols), BF16),
         pltpu.VMEM((chunks, rows_c // 2, cols), BF16),
@@ -564,25 +651,27 @@
     )(*small, *large)
 
 
-def routing(route_ids, route_weights, experts, capacity):
-    tokens = route_ids.shape[0]
-    ids = route_ids.T
-    weights = route_weights.T
-    names = lax.broadcasted_iota(jnp.int32, (experts, tokens), 0)
-    first, second = names == ids[0][None, :], names == ids[1][None, :]
-    weight = jnp.where(first, weights[0][None, :], 0.0) + jnp.where(
-        second, weights[1][None, :], 0.0
-    )
-    named = first | second
-    earlier = lax.broadcasted_iota(jnp.int32, (tokens, tokens), 0) < lax.broadcasted_iota(
-        jnp.int32, (tokens, tokens), 1
-    )
-    rank = jnp.dot(named.astype(BF16), earlier.astype(BF16), preferred_element_type=F32)
-    rank = jnp.where(named, rank.astype(jnp.int32), -1)
-    slots = lax.broadcasted_iota(jnp.int32, (experts, capacity, tokens), 1)
-    chosen = rank[:, None, :] == slots
-    slot_weight = jnp.sum(jnp.where(chosen, weight[:, None, :], 0.0), axis=2)
-    return chosen.reshape(experts * capacity, tokens).astype(BF16), slot_weight.reshape(-1, 1)
+def store_kernel(count, *refs):
+    sems = refs[-1]
+    copies = [
+        pltpu.make_async_copy(refs[n], refs[count + n], sems.at[n]) for n in range(count)
+    ]
+    for copy in copies:
+        copy.start()
+    for copy in copies:
+        copy.wait()
+
+
+def store(values):
+    count = len(values)
+    return pl.pallas_call(
+        functools.partial(store_kernel, count),
+        out_shape=tuple(jax.ShapeDtypeStruct(v.shape, v.dtype) for v in values),
+        in_specs=[pl.BlockSpec(memory_space=pltpu.VMEM)] * count,
+        out_specs=(pl.BlockSpec(memory_space=pltpu.HBM),) * count,
+        scratch_shapes=[pltpu.SemaphoreType.DMA((count,))],
+        name="store",
+    )(*values)
 
 
 def body(
@@ -604,19 +693,12 @@
     groups = lax.axis_size("sp")
     lanes = lax.axis_size("tp")
     capacity = expert_inputs.shape[1] // groups
-    experts = groups
-    model_width = cotangent.shape[1]
-    lane_cols = model_width // lanes
-    own_rows = lax.dynamic_slice_in_dim(cotangent, lax.axis_index("tp") * lane_cols, lane_cols, 1)
-    chosen, slot_weight = routing(route_ids, route_weights, experts, capacity)
-    picked = jnp.dot(chosen, own_rows, preferred_element_type=F32)
-    outgoing = (slot_weight * picked).astype(BF16)
-    grad_input, grad_gate, grad_up, grad_down, *rest = run_step(
+    results = run_step(
         (groups, lanes, chunks, capacity),
         (
-            outgoing,
-            chosen,
-            own_rows,
+            route_ids.T,
+            route_weights.T,
+            cotangent,
             out_weight,
             gate_in,
             conv_sum,
@@ -626,6 +708,7 @@
         ),
         (expert_inputs[0], gate_weight[0], up_weight[0], down_weight[0]),
     )
+    grad_input, grad_gate, grad_up, grad_down, *rest = store(results)
     return (grad_input, grad_gate[None], grad_up[None], grad_down[None], *rest)
 
 
@@ -645,7 +728,7 @@
         P("sp", "tp"),
         P(None, "tp"),
     )
-    chunks = min(8, mesh.shape["sp"] // 2)
+    chunks = 8
     return jax.shard_map(
         functools.partial(body, chunks),
         mesh=mesh,

time: 145 us -> 126 us (0.87)
  local copies, waits for them, and re-layouts: 10.3 us -> 0 us
  Pallas kernels: 130 us -> 125 us
  matrix products: 1.58 us -> 0 us
    pallas_call x1, Pallas kernels: 130 us -> 121 us  [run_step(): pl.pallas_call(functools.partial(step_kernel, dims), out_shape=tuple((jax...]
    unnamed x24 -> x0, local copies, waits for them, and re-layouts: 8.58 us -> none
    pallas_call x0 -> x1, Pallas kernels: none -> 3.84 us  [store(): pl.pallas_call(functools.partial(store_kernel, count), out_shape=tuple((j...]
    dot_general x2 -> x0, matrix products: 1.58 us -> none  [the longest x1 1.41 us: body(): picked = jnp.dot(chosen, own_rows, preferred_element_type=F32)]
    slice x2 -> x0, local copies, waits for them, and re-layouts: 1.55 us -> none  [the longest x1 0.79 us: routing(): first, second = (names == ids[0][None, :], names == ids[1][None, :])]
where the time goes in v3:
time: 126 us
  Pallas kernels  125 us (99%)
    pallas_call x1, Pallas kernels, run_step(): pl.pallas_call(functools.partial(step_kernel, dims), out_shape=tuple((jax...  121 us
    pallas_call x1, Pallas kernels, store(): pl.pallas_call(functools.partial(store_kernel, count), out_shape=tuple((j...  3.84 us

profile of v3, /device:TPU:17, one launch (start us, length us, event | category | flops | bytes accessed | tf_op | source)
XLA Modules:
  0.0 125.5 jit_solution(8720681998365730022)
XLA Ops:
  0.6 121.0 %step.1 = (bf16[256,512]{1,0:T(8,128)(2,1)}, bf16[2048,256]{1,0:T(8,128)(2,1)}, bf16[2048,256]{1,0:T(8,128)(2,1)}, bf16[256,2048]{1,0:T(8,128)(2,1)}, f32[32,128...) custom-call(s32[2,256]{1,0:T(2,128)} %bitcast.13, ...), custom_call_target="tpu_custom_call" | custom-call | tf_op jit(solution)/shard_map/step/pallas_call | solution.py:641
  121.7 3.8 %store.1 = (bf16[256,512]{1,0:T(8,128)(2,1)}, bf16[2048,256]{1,0:T(8,128)(2,1)}, bf16[2048,256]{1,0:T(8,128)(2,1)}, bf16[256,2048]{1,0:T(8,128)(2,1)}, f32[32,12...) custom-call(bf16[256,512]{1,0:T(8,128)(2,1)} %get-tuple-element.24.refs_0_, ...), custom_call_target="tpu_custom_call" | custom-call | tf_op jit(solution)/shard_map/store/pallas_call | solution.py:667

commit v4 on v3

--- a/solution.py
+++ b/solution.py
@@ -28,9 +28,9 @@
     up_hbm,
     down_hbm,
     grad_input,
-    g_gate,
-    g_up,
-    g_down,
+    g_gate_hbm,
+    g_up_hbm,
+    g_down_hbm,
     g_out,
     g_gate_in,
     g_conv_c,
@@ -46,6 +46,9 @@
     sums,
     out_terms,
     out_in,
+    g_gate,
+    g_up,
+    g_down,
     x_v,
     gate_v,
     up_v,
@@ -63,6 +66,7 @@
     gpg_s,
     gpu_s,
     load_sem,
+    store_sem,
     send_z,
     recv_z,
     send_y,
@@ -132,15 +136,15 @@
         jnp.where(pick, weight[:, None, :], 0.0).reshape(rows_all, tokens), axis=1, keepdims=True
     )
     lane_span = pl.ds(pl.multiple_of(q * cols, cols), cols)
-    for slot, step_z in enumerate((0, 1, chunks - 1)):
+
+    def build_near(slot, step_z):
         rows = pl.ds(pl.multiple_of(((z + step_z) % chunks) * rows_c, rows_c), rows_c)
         near_ref[slot * rows_c : (slot + 1) * rows_c, :] = (
             slot_weight[rows, :]
             * jnp.dot(chosen[rows, :], cot[...], preferred_element_type=F32)
         ).astype(BF16)
-    out_ref[...] = (
-        slot_weight[...] * jnp.dot(chosen[...], cot[:, lane_span], preferred_element_type=F32)
-    ).astype(BF16)
+
+    build_near(0, 0)
     pl.semaphore_wait(barrier, sps - 1 + 2)
 
     far_last = chunks - near
@@ -202,8 +206,12 @@
         return lax.fori_loop(0, group, send_one, carry)
 
     lax.fori_loop(1, group, send_own, 0)
-    lax.fori_loop(1, far_last + 1, send_far, 0)
-    lax.fori_loop(far_last + 1, chunks, send_near, 0)
+    out_ref[...] = (
+        slot_weight[...] * jnp.dot(chosen[...], cot[:, lane_span], preferred_element_type=F32)
+    ).astype(BF16)
+    lax.fori_loop(1, 3+1, send_far, 0)
+    build_near(1, 1)
+    build_near(2, chunks - 1)
     routed[own, :] = near_ref[pl.ds(pl.multiple_of(g * cap, cap), cap), :]
 
     chosen_t[...] = chosen[...].T
@@ -293,6 +301,14 @@
         far_block(i).wait_recv()
         gather_up(i).start()
         gather_dn(i).start()
+
+        @pl.when(i + 3 <= far_last)
+        def _():
+            send_far(i + 3, 0)
+
+        @pl.when((i + 3 > far_last) & (i + 3 < chunks))
+        def _():
+            send_near(i + 3, 0)
 
     def stage_pass(i):
         gather_up(i).wait_recv()
@@ -414,53 +430,70 @@
         device_id=(me, up_q),
         device_id_type=MESH,
     )
+    contract0 = (((0,), (0,)), ((), ()))
+    stores = [
+        pltpu.make_async_copy(src, dst, store_sem.at[n])
+        for n, (src, dst) in enumerate(
+            ((g_down, g_down_hbm), (g_gate, g_gate_hbm), (g_up, g_up_hbm))
+        )
+    ]
+    for lane in range(tps):
+        span = slice(lane * cols, (lane + 1) * cols)
+        g_down[:, span] = lax.dot_general(
+            hidden_s[...], routed[:, span], contract0, preferred_element_type=F32
+        ).astype(BF16)
+    stores[0].start()
+    for lane in range(tps):
+        span = slice(lane * cols, (lane + 1) * cols)
+        g_gate[span, :] = lax.dot_general(
+            x_v[:, span], gpg_s[...], contract0, preferred_element_type=F32
+        ).astype(BF16)
+    stores[1].start()
     final.wait_recv()
 
-    own_grad = (
-        cot[:, lane_span].astype(F32)
-        + jnp.dot(chosen_t[...], returned[...], preferred_element_type=F32)
-    ).astype(BF16)
-    grad_input[...] = own_grad
-    full_in[q] = own_grad
-
-    def share(lane, first, size, kind, peer):
-        ref = full_in.at[lane, pl.ds(first, size), :]
+    pieces = 2
+    wide = cols // pieces
+    split = tokens // 2
+
+    def share(lane, piece, first, size, kind, peer):
+        ref = full_in.at[lane, pl.ds(first, size), pl.ds(piece * wide, wide)]
         return pltpu.make_async_remote_copy(
             src_ref=ref,
             dst_ref=ref,
-            send_sem=send_s.at[kind],
-            recv_sem=recv_s.at[kind],
+            send_sem=send_s.at[kind, piece],
+            recv_sem=recv_s.at[kind, piece],
             device_id=(me, peer),
             device_id_type=MESH,
         )
 
-    split = tokens // 2
-    shares = (
-        share(q, 0, tokens, 0, up_q),
-        share(q, 0, tokens, 1, dn_q),
-        share(dn_q, 0, split, 2, up_q),
-        share(up_q, split, split, 3, dn_q),
-    )
-    shares[0].start()
-    shares[1].start()
-
-    contract0 = (((0,), (0,)), ((), ()))
+    shares = [
+        (
+            share(q, piece, 0, tokens, 0, up_q),
+            share(q, piece, 0, tokens, 1, dn_q),
+            share(dn_q, piece, 0, split, 2, up_q),
+            share(up_q, piece, split, split, 3, dn_q),
+        )
+        for piece in range(pieces)
+    ]
     per_lane = sps // tps
+    per_piece = per_lane // pieces
     owned = g_out.shape[0]
 
-    def send_terms(lane):
-        out_terms[lane] = lax.dot_general(
-            full_in[lane], mixed[...], contract0, preferred_element_type=F32
+    def send_terms(lane, piece):
+        span = slice(piece * wide, (piece + 1) * wide)
+        out_terms[lane, span, :] = lax.dot_general(
+            full_in[lane, :, span], mixed[...], contract0, preferred_element_type=F32
         ).astype(BF16)
 
         def send_one(k, carry):
-            place = (g + k) % per_lane
+            place = piece * per_piece + (g + k) % per_piece
             owner = lane * per_lane + place
+            block = pl.ds(pl.multiple_of(place * owned, owned), owned)
 
             @pl.when(owner != me)
             def _():
                 pltpu.make_async_remote_copy(
-                    src_ref=out_terms.at[lane, pl.ds(pl.multiple_of(place * owned, owned), owned), :],
+                    src_ref=out_terms.at[lane, block, :],
                     dst_ref=out_in.at[me],
                     send_sem=send_o,
                     recv_sem=recv_o,
@@ -470,35 +503,43 @@
 
             @pl.when(owner == me)
             def _():
-                out_in[me] = out_terms[lane, pl.ds(pl.multiple_of(place * owned, owned), owned), :]
+                out_in[me] = out_terms[lane, block, :]
 
             return carry
 
-        lax.fori_loop(0, per_lane, send_one, 0)
-
-    send_terms(q)
-
+        lax.fori_loop(0, per_piece, send_one, 0)
+
+    for piece in range(pieces):
+        span = slice(piece * wide, (piece + 1) * wide)
+        own_cols = pl.ds(pl.multiple_of(q * cols + piece * wide, wide), wide)
+        own_grad = (
+            cot[:, own_cols].astype(F32)
+            + jnp.dot(chosen_t[...], returned[:, span], preferred_element_type=F32)
+        ).astype(BF16)
+        grad_input[:, span] = own_grad
+        full_in[q, :, span] = own_grad
+        shares[piece][0].start()
+        shares[piece][1].start()
+    for piece in range(pieces):
+        send_terms(q, piece)
     for lane in range(tps):
         span = slice(lane * cols, (lane + 1) * cols)
-        g_down[:, span] = lax.dot_general(
-            hidden_s[...], routed[:, span], contract0, preferred_element_type=F32
-        ).astype(BF16)
-        g_gate[span, :] = lax.dot_general(
-            x_v[:, span], gpg_s[...], contract0, preferred_element_type=F32
-        ).astype(BF16)
         g_up[span, :] = lax.dot_general(
             x_v[:, span], gpu_s[...], contract0, preferred_element_type=F32
         ).astype(BF16)
-
-    shares[0].wait_recv()
-    shares[2].start()
-    shares[1].wait_recv()
-    shares[3].start()
-    send_terms(dn_q)
-    send_terms(up_q)
-    shares[2].wait_recv()
-    shares[3].wait_recv()
-    send_terms(far_q)
+    stores[2].start()
+
+    for piece in range(pieces):
+        shares[piece][0].wait_recv()
+        shares[piece][2].start()
+        shares[piece][1].wait_recv()
+        shares[piece][3].start()
+        send_terms(dn_q, piece)
+        send_terms(up_q, piece)
+    for piece in range(pieces):
+        shares[piece][2].wait_recv()
+        shares[piece][3].wait_recv()
+        send_terms(far_q, piece)
 
     grad_mixed = jnp.zeros((tokens, out_weight.shape[1]), F32)
     for lane in range(tps):
@@ -547,8 +588,11 @@
 
     terms.wait_send()
     shift.wait_send()
-    for copy in shares:
-        copy.wait_send()
+    for row in shares:
+        for copy in row:
+            copy.wait_send()
+    for copy in stores:
+        copy.wait()
 
     def drain_far(i, carry):
         for copy in every[:4]:
@@ -598,6 +642,9 @@
         pltpu.VMEM((tokens + 8, lane_w), F32),
         pltpu.VMEM((tps, cols, lane_w), BF16),
         pltpu.VMEM((sps, width // sps, lane_w), BF16),
+        pltpu.VMEM((width, units), BF16),
+        pltpu.VMEM((width, units), BF16),
+        pltpu.VMEM((units, width), BF16),
         pltpu.VMEM((rows, width), BF16),
         pltpu.VMEM((width, units), BF16),
         pltpu.VMEM((width, units), BF16),
@@ -615,14 +662,15 @@
         pltpu.VMEM((rows, units), BF16),
         pltpu.VMEM((rows, units), BF16),
         dma((4,)),
+        dma((3,)),
         dma((chunks,)),
         dma((chunks,)),
         dma((8, chunks)),
         dma((8, chunks)),
         dma,
         dma,
-        dma((4,)),
-        dma((4,)),
+        dma((4, 2)),
+        dma((4, 2)),
         dma,
         dma,
         dma,
@@ -642,7 +690,7 @@
         functools.partial(step_kernel, dims),
         out_shape=tuple(jax.ShapeDtypeStruct(*out) for out in outs),
         in_specs=[vmem] * len(small) + [hbm] * len(large),
-        out_specs=(vmem,) * len(outs),
+        out_specs=(vmem, hbm, hbm, hbm, vmem, vmem, vmem, vmem),
         scratch_shapes=scratch,
         compiler_params=pltpu.CompilerParams(
             collective_id=0, has_side_effects=True, vmem_limit_bytes=60 * 1024 * 1024
@@ -652,24 +700,31 @@
 
 
 def store_kernel(count, *refs):
-    sems = refs[-1]
-    copies = [
-        pltpu.make_async_copy(refs[n], refs[count + n], sems.at[n]) for n in range(count)
-    ]
-    for copy in copies:
-        copy.start()
-    for copy in copies:
-        copy.wait()
+    given, results, held = refs[:count], refs[count : 2 * count], refs[2 * count : 3 * count]
+    load_sem, store_sem = refs[3 * count :]
+    loads = [pltpu.make_async_copy(given[n], held[n], load_sem.at[n]) for n in range(count)]
+    stores = [pltpu.make_async_copy(held[n], results[n], store_sem.at[n]) for n in range(count)]
+    for load in loads:
+        load.start()
+    for load, out in zip(loads, stores):
+        load.wait()
+        out.start()
+    for out in stores:
+        out.wait()
 
 
 def store(values):
     count = len(values)
+    hbm = pl.BlockSpec(memory_space=pltpu.HBM)
+    dma = pltpu.SemaphoreType.DMA
     return pl.pallas_call(
         functools.partial(store_kernel, count),
         out_shape=tuple(jax.ShapeDtypeStruct(v.shape, v.dtype) for v in values),
-        in_specs=[pl.BlockSpec(memory_space=pltpu.VMEM)] * count,
-        out_specs=(pl.BlockSpec(memory_space=pltpu.HBM),) * count,
-        scratch_shapes=[pltpu.SemaphoreType.DMA((count,))],
+        in_specs=[hbm] * count,
+        out_specs=(hbm,) * count,
+        scratch_shapes=[pltpu.VMEM(v.shape, v.dtype) for v in values]
+        + [dma((count,)), dma((count,))],
+        compiler_params=pltpu.CompilerParams(vmem_limit_bytes=60 * 1024 * 1024),
         name="store",
     )(*values)
 

time: 126 us -> 120 us (0.952)
  Pallas kernels: 125 us -> 119 us
    pallas_call x1, Pallas kernels: 121 us -> 116 us  [run_step(): pl.pallas_call(functools.partial(step_kernel, dims), out_shape=tuple((jax...]
where the time goes in v4:
time: 120 us
  Pallas kernels  119 us (99%)
    pallas_call x1, Pallas kernels, run_step(): pl.pallas_call(functools.partial(step_kernel, dims), out_shape=tuple((jax...  116 us
    pallas_call x1, Pallas kernels, store(): pl.pallas_call(functools.partial(store_kernel, count), out_shape=tuple((j...  3.2 us

profile of v4, /device:TPU:17, one launch (start us, length us, event | category | flops | bytes accessed | tf_op | source)
XLA Modules:
  0.0 120.0 jit_solution(1934506980638839648)
XLA Ops:
  0.6 116.1 %step.1 = (bf16[256,512]{1,0:T(8,128)(2,1)}, bf16[2048,256]{1,0:T(8,128)(2,1)}, bf16[2048,256]{1,0:T(8,128)(2,1)}, bf16[256,2048]{1,0:T(8,128)(2,1)}, f32[32,128...) custom-call(s32[2,256]{1,0:T(2,128)} %bitcast.13, ...), custom_call_target="tpu_custom_call" | custom-call | tf_op jit(solution)/shard_map/step/pallas_call | solution.py:689
  116.8 3.2 %store.1 = (bf16[256,512]{1,0:T(8,128)(2,1)}, bf16[2048,256]{1,0:T(8,128)(2,1)}, bf16[2048,256]{1,0:T(8,128)(2,1)}, bf16[256,2048]{1,0:T(8,128)(2,1)}, f32[32,12...) custom-call(bf16[256,512]{1,0:T(8,128)(2,1)} %get-tuple-element.24.refs_0_, ...), custom_call_target="tpu_custom_call" | custom-call | tf_op jit(solution)/shard_map/store/pallas_call | solution.py:720

commit v5 on v4

--- a/solution.py
+++ b/solution.py
@@ -81,7 +81,7 @@
     recv_n,
 ):
     sps, tps, chunks, cap = dims
-    near = 3
+    near = 2
     group = sps // chunks
     rows_c = group * cap
     half = rows_c // 2
@@ -144,10 +144,12 @@
             * jnp.dot(chosen[rows, :], cot[...], preferred_element_type=F32)
         ).astype(BF16)
 
-    build_near(0, 0)
+    out_ref[...] = (
+        slot_weight[...] * jnp.dot(chosen[...], cot[:, lane_span], preferred_element_type=F32)
+    ).astype(BF16)
     pl.semaphore_wait(barrier, sps - 1 + 2)
 
-    far_last = chunks - near
+    far_last = chunks - near - 1
 
     def offset(i):
         u = (i + chunks - 1) % chunks
@@ -188,7 +190,7 @@
         )
 
     def send_own(k, carry):
-        near_copy(0, 0, k).start()
+        far_copy(0, k).start()
         return carry
 
     def send_far(i, carry):
@@ -200,19 +202,16 @@
 
     def send_near(i, carry):
         def send_one(k, inner):
-            near_copy(i, i - far_last, k).start()
+            near_copy(i, i - far_last - 1, k).start()
             return inner
 
         return lax.fori_loop(0, group, send_one, carry)
 
     lax.fori_loop(1, group, send_own, 0)
-    out_ref[...] = (
-        slot_weight[...] * jnp.dot(chosen[...], cot[:, lane_span], preferred_element_type=F32)
-    ).astype(BF16)
-    lax.fori_loop(1, 3+1, send_far, 0)
-    build_near(1, 1)
-    build_near(2, chunks - 1)
-    routed[own, :] = near_ref[pl.ds(pl.multiple_of(g * cap, cap), cap), :]
+    lax.fori_loop(1, 4, send_far, 0)
+    routed[own, lane_span] = out_ref[own, :]
+    build_near(0, 1)
+    build_near(1, chunks - 1)
 
     chosen_t[...] = chosen[...].T
     mixed[...] = (gate_in[...].astype(F32) * conv_sum[...].astype(F32)).astype(BF16)
@@ -276,18 +275,19 @@
 
     every = (gather_up, gather_dn, pass_up, pass_dn, first_up, first_dn, last_up, last_dn)
 
-    def far_block(i):
+    def far_block(i, count):
+        rows = pl.ds(0, count * cap)
         return pltpu.make_async_remote_copy(
-            src_ref=out_ref.at[pl.ds(0, rows_c), :],
-            dst_ref=routed.at[pl.ds(0, rows_c), lane_span],
+            src_ref=out_ref.at[rows, :],
+            dst_ref=routed.at[rows, lane_span],
             send_sem=send_z.at[i],
             recv_sem=recv_z.at[i],
             device_id=(me, up_q),
             device_id_type=MESH,
         )
 
-    def near_block(i, count):
-        rows = pl.ds(0, count * cap)
+    def near_block(i):
+        rows = pl.ds(0, rows_c)
         return pltpu.make_async_remote_copy(
             src_ref=near_ref.at[rows, :],
             dst_ref=routed.at[rows, :],
@@ -298,11 +298,20 @@
         )
 
     def stage_gather(i):
-        far_block(i).wait_recv()
+        if group > 1:
+
+            @pl.when(i == 0)
+            def _():
+                far_block(0, group - 1).wait_recv()
+
+        @pl.when(i > 0)
+        def _():
+            far_block(i, group).wait_recv()
+
         gather_up(i).start()
         gather_dn(i).start()
 
-        @pl.when(i + 3 <= far_last)
+        @pl.when((i > 0) & (i + 3 <= far_last))
         def _():
             send_far(i + 3, 0)
 
@@ -350,7 +359,7 @@
 
         @pl.when(i > far_last)
         def _():
-            near_block(i, group).wait_recv()
+            near_block(i).wait_recv()
 
         compute(i)
 
@@ -396,20 +405,15 @@
         lax.fori_loop(1, group, send_one, 0)
 
     forward(0)
-    if group > 1:
-        near_block(0, group - 1).wait_recv()
-    compute(0)
-    forward(1)
-    stage_first(0)
 
     def step(t, carry):
         for stage, lead, first, last in (
-            (stage_gather, 1, 1, far_last),
-            (stage_pass, 0, 1, far_last),
-            (stage_compute, -1, 1, chunks - 1),
-            (forward, 2, 2, chunks - 1),
-            (stage_first, -2, 1, chunks - 1),
-            (stage_return, -3, 0, chunks - 1),
+            (stage_gather, 0, 0, far_last),
+            (stage_pass, -1, 0, far_last),
+            (stage_compute, -2, 0, chunks - 1),
+            (forward, 1, 1, chunks - 1),
+            (stage_first, -3, 0, chunks - 1),
+            (stage_return, -4, 0, chunks - 1),
         ):
             i = t + lead
 
@@ -419,7 +423,7 @@
 
         return carry
 
-    lax.fori_loop(0, chunks + 3, step, 0)
+    lax.fori_loop(0, chunks + 4, step, 0)
     returned[own, :] = ret_src[own, :]
     rest = pl.ds(0, (sps - 1) * cap)
     final = pltpu.make_async_remote_copy(
@@ -451,7 +455,7 @@
     stores[1].start()
     final.wait_recv()
 
-    pieces = 2
+    pieces = 4
     wide = cols // pieces
     split = tokens // 2
 
@@ -597,7 +601,11 @@
     def drain_far(i, carry):
         for copy in every[:4]:
             copy(i).wait_send()
-        far_block(i).wait_send()
+
+        @pl.when(i > 0)
+        def _():
+            far_block(i, group).wait_send()
+
         return carry
 
     def drain_sum(i, carry):
@@ -606,14 +614,14 @@
         return carry
 
     def drain_near(i, carry):
-        near_block(i, group).wait_send()
+        near_block(i).wait_send()
         return carry
 
-    lax.fori_loop(1, far_last + 1, drain_far, 0)
+    lax.fori_loop(0, far_last + 1, drain_far, 0)
     lax.fori_loop(0, chunks, drain_sum, 0)
     lax.fori_loop(far_last + 1, chunks, drain_near, 0)
     if group > 1:
-        near_block(0, group - 1).wait_send()
+        far_block(0, group - 1).wait_send()
     final.wait_send()
 
 
@@ -632,7 +640,7 @@
     dma = pltpu.SemaphoreType.DMA
     scratch = [
         pltpu.VMEM((rows, cols), BF16),
-        pltpu.VMEM((3 * rows_c, width), BF16),
+        pltpu.VMEM((2 * rows_c, width), BF16),
         pltpu.VMEM((rows, tokens), BF16),
         pltpu.VMEM((rows, 1), F32),
         pltpu.VMEM((rows, cols), BF16),
@@ -669,8 +677,8 @@
         dma((8, chunks)),
         dma,
         dma,
-        dma((4, 2)),
-        dma((4, 2)),
+        dma((4, 4)),
+        dma((4, 4)),
         dma,
         dma,
         dma,

time: 120 us -> 116 us (0.967)
  Pallas kernels: 119 us -> 115 us
    pallas_call x1, Pallas kernels: 116 us -> 112 us  [run_step(): pl.pallas_call(functools.partial(step_kernel, dims), out_shape=tuple((jax...]
where the time goes in v5:
time: 116 us; the launch traced here: 115 us
  Pallas kernels  115 us (99%)
    pallas_call x1, Pallas kernels, run_step(): pl.pallas_call(functools.partial(step_kernel, dims), out_shape=tuple((jax...  112 us
    pallas_call x1, Pallas kernels, store(): pl.pallas_call(functools.partial(store_kernel, count), out_shape=tuple((j...  3.2 us

profile of v5, /device:TPU:17, one launch (start us, length us, event | category | flops | bytes accessed | tf_op | source)
XLA Modules:
  0.0 115.4 jit_solution(8751388828211818612)
XLA Ops:
  0.6 111.6 %step.1 = (bf16[256,512]{1,0:T(8,128)(2,1)}, bf16[2048,256]{1,0:T(8,128)(2,1)}, bf16[2048,256]{1,0:T(8,128)(2,1)}, bf16[256,2048]{1,0:T(8,128)(2,1)}, f32[32,128...) custom-call(s32[2,256]{1,0:T(2,128)} %bitcast.13, ...), custom_call_target="tpu_custom_call" | custom-call | tf_op jit(solution)/shard_map/step/pallas_call | solution.py:697
  112.2 3.2 %store.1 = (bf16[256,512]{1,0:T(8,128)(2,1)}, bf16[2048,256]{1,0:T(8,128)(2,1)}, bf16[2048,256]{1,0:T(8,128)(2,1)}, bf16[256,2048]{1,0:T(8,128)(2,1)}, f32[32,12...) custom-call(bf16[256,512]{1,0:T(8,128)(2,1)} %get-tuple-element.24.refs_0_, ...), custom_call_target="tpu_custom_call" | custom-call | tf_op jit(solution)/shard_map/store/pallas_call | solution.py:728

commit v6 on v5

--- a/solution.py
+++ b/solution.py
@@ -17,20 +17,30 @@
     ids,
     weights,
     cot,
+    taps,
+    out_weight_hbm,
+    gate_in_hbm,
+    conv_sum_hbm,
+    conv_c_hbm,
+    conv_v_hbm,
+    x_hbm,
+    gate_hbm,
+    up_hbm,
+    down_hbm,
+    grad_input_hbm,
+    g_gate_hbm,
+    g_up_hbm,
+    g_down_hbm,
+    g_out_hbm,
+    g_gate_in_hbm,
+    g_conv_c_hbm,
+    g_conv_v_hbm,
     out_weight,
     gate_in,
     conv_sum,
     conv_c,
     conv_v,
-    taps,
-    x_hbm,
-    gate_hbm,
-    up_hbm,
-    down_hbm,
     grad_input,
-    g_gate_hbm,
-    g_up_hbm,
-    g_down_hbm,
     g_out,
     g_gate_in,
     g_conv_c,
@@ -99,7 +109,17 @@
     loads = [
         pltpu.make_async_copy(src, dst, load_sem.at[n])
         for n, (src, dst) in enumerate(
-            ((x_hbm, x_v), (gate_hbm, gate_v), (up_hbm, up_v), (down_hbm, down_v))
+            (
+                (x_hbm, x_v),
+                (gate_hbm, gate_v),
+                (up_hbm, up_v),
+                (down_hbm, down_v),
+                (gate_in_hbm, gate_in),
+                (conv_sum_hbm, conv_sum),
+                (conv_c_hbm, conv_c),
+                (conv_v_hbm, conv_v),
+                (out_weight_hbm, out_weight),
+            )
         )
     ]
     for load in loads:
@@ -214,10 +234,10 @@
     build_near(1, chunks - 1)
 
     chosen_t[...] = chosen[...].T
-    mixed[...] = (gate_in[...].astype(F32) * conv_sum[...].astype(F32)).astype(BF16)
 
     for load in loads:
         load.wait()
+    mixed[...] = (gate_in[...].astype(F32) * conv_sum[...].astype(F32)).astype(BF16)
 
     def at(i, first=0, size=None):
         return pl.ds(pl.multiple_of(chunk_start(i) + first, half), size or rows_c)
@@ -438,7 +458,16 @@
     stores = [
         pltpu.make_async_copy(src, dst, store_sem.at[n])
         for n, (src, dst) in enumerate(
-            ((g_down, g_down_hbm), (g_gate, g_gate_hbm), (g_up, g_up_hbm))
+            (
+                (g_down, g_down_hbm),
+                (g_gate, g_gate_hbm),
+                (g_up, g_up_hbm),
+                (grad_input, grad_input_hbm),
+                (g_gate_in, g_gate_in_hbm),
+                (g_conv_c, g_conv_c_hbm),
+                (g_conv_v, g_conv_v_hbm),
+                (g_out, g_out_hbm),
+            )
         )
     ]
     for lane in range(tps):
@@ -524,6 +553,7 @@
         full_in[q, :, span] = own_grad
         shares[piece][0].start()
         shares[piece][1].start()
+    stores[3].start()
     for piece in range(pieces):
         send_terms(q, piece)
     for lane in range(tps):
@@ -564,6 +594,7 @@
     )
     shift.start()
     g_gate_in[...] = (grad_mixed * conv_sum[...].astype(F32)).astype(BF16)
+    stores[4].start()
     shift.wait_recv()
 
     @pl.when(me == sps - 1)
@@ -577,6 +608,8 @@
     )
     g_conv_c[...] = (grad_prod * conv_v[...].astype(F32)).astype(BF16)
     g_conv_v[...] = (grad_prod * conv_c[...].astype(F32)).astype(BF16)
+    stores[5].start()
+    stores[6].start()
 
     others = out_in.at[pl.ds(0, sps - 1)]
     terms = pltpu.make_async_remote_copy(
@@ -589,6 +622,7 @@
     )
     terms.wait_recv()
     g_out[...] = jnp.sum(out_in[...].astype(F32), axis=0)
+    stores[7].start()
 
     terms.wait_send()
     shift.wait_send()
@@ -627,8 +661,8 @@
 
 def run_step(dims, small, large):
     sps, tps, chunks, cap = dims
-    cot, out_weight = small[2:4]
-    gate = large[1]
+    cot, out_weight = small[2], large[0]
+    gate = large[6]
     rows = sps * cap
     tokens = cot.shape[0]
     cols = cot.shape[1] // tps
@@ -638,7 +672,18 @@
     vmem = pl.BlockSpec(memory_space=pltpu.VMEM)
     hbm = pl.BlockSpec(memory_space=pltpu.HBM)
     dma = pltpu.SemaphoreType.DMA
+    lane_bf16 = pltpu.VMEM((tokens, lane_w), BF16)
     scratch = [
+        pltpu.VMEM((width, lane_w), BF16),
+        lane_bf16,
+        lane_bf16,
+        lane_bf16,
+        lane_bf16,
+        pltpu.VMEM((tokens, cols), BF16),
+        pltpu.VMEM((width // sps, lane_w), F32),
+        lane_bf16,
+        lane_bf16,
+        lane_bf16,
         pltpu.VMEM((rows, cols), BF16),
         pltpu.VMEM((2 * rows_c, width), BF16),
         pltpu.VMEM((rows, tokens), BF16),
@@ -669,8 +714,8 @@
         pltpu.VMEM((rows, units), BF16),
         pltpu.VMEM((rows, units), BF16),
         pltpu.VMEM((rows, units), BF16),
-        dma((4,)),
-        dma((3,)),
+        dma((9,)),
+        dma((8,)),
         dma((chunks,)),
         dma((chunks,)),
         dma((8, chunks)),
@@ -698,7 +743,7 @@
         functools.partial(step_kernel, dims),
         out_shape=tuple(jax.ShapeDtypeStruct(*out) for out in outs),
         in_specs=[vmem] * len(small) + [hbm] * len(large),
-        out_specs=(vmem, hbm, hbm, hbm, vmem, vmem, vmem, vmem),
+        out_specs=(hbm,) * len(outs),
         scratch_shapes=scratch,
         compiler_params=pltpu.CompilerParams(
             collective_id=0, has_side_effects=True, vmem_limit_bytes=60 * 1024 * 1024
@@ -758,18 +803,18 @@
     capacity = expert_inputs.shape[1] // groups
     results = run_step(
         (groups, lanes, chunks, capacity),
+        (route_ids.T, route_weights.T, cotangent, conv_taps),
         (
-            route_ids.T,
-            route_weights.T,
-            cotangent,
             out_weight,
             gate_in,
             conv_sum,
             conv_c,
             conv_v,
-            conv_taps,
+            expert_inputs[0],
+            gate_weight[0],
+            up_weight[0],
+            down_weight[0],
         ),
-        (expert_inputs[0], gate_weight[0], up_weight[0], down_weight[0]),
     )
     grad_input, grad_gate, grad_up, grad_down, *rest = store(results)
     return (grad_input, grad_gate[None], grad_up[None], grad_down[None], *rest)

time: 116 us -> 116 us (level)
  no operation moved by 1% of the time
where the time goes in v6:
time: 116 us; the launch traced here: 115 us
  Pallas kernels  114 us (98%)
    pallas_call x1, Pallas kernels, run_step(): pl.pallas_call(functools.partial(step_kernel, dims), out_shape=tuple((jax...  111 us
    pallas_call x1, Pallas kernels, store(): pl.pallas_call(functools.partial(store_kernel, count), out_shape=tuple((j...  3.2 us

profile of v6, /device:TPU:17, one launch (start us, length us, event | category | flops | bytes accessed | tf_op | source)
XLA Modules:
  0.0 114.8 jit_solution(4627645366656696205)
XLA Ops:
  0.6 110.9 %step.1 = (bf16[256,512]{1,0:T(8,128)(2,1)}, bf16[2048,256]{1,0:T(8,128)(2,1)}, bf16[2048,256]{1,0:T(8,128)(2,1)}, bf16[256,2048]{1,0:T(8,128)(2,1)}, f32[32,128...) custom-call(s32[2,256]{1,0:T(2,128)} %bitcast.13, ...), custom_call_target="tpu_custom_call" | custom-call | tf_op jit(solution)/shard_map/step/pallas_call | solution.py:742
  111.6 3.2 %store.1 = (bf16[256,512]{1,0:T(8,128)(2,1)}, bf16[2048,256]{1,0:T(8,128)(2,1)}, bf16[2048,256]{1,0:T(8,128)(2,1)}, bf16[256,2048]{1,0:T(8,128)(2,1)}, f32[32,12...) custom-call(bf16[256,512]{1,0:T(8,128)(2,1)} %get-tuple-element.24.refs_0_, ...), custom_call_target="tpu_custom_call" | custom-call | tf_op jit(solution)/shard_map/store/pallas_call | solution.py:773
